TPU v7x, 256 devices: a whole 4x4x8 slice. The times are simulated.
256 devices in a mesh: kv: 32 (over z, x), tp: 8 (over y, core).
Axes of the slice: x: 4, y: 4, z: 8, core: 2. Of those that a mesh axis runs over, the one named last changes fastest.
Arguments:
- tokens: bfloat16 [384, 2048], P('tp', 'kv'), may hold values from -10.5 to 10.5
- norm_gain: float32 [2048], P('kv'), may hold values from 0.1 to 1.9
- w_query: bfloat16 [2048, 2048], P('kv', 'tp'), may hold values from -0.125 to 0.125
- w_forget: bfloat16 [2048, 2048], P('kv', 'tp'), may hold values from -0.125 to 0.125
- w_input: bfloat16 [2048, 2048], P('kv', 'tp'), may hold values from -0.125 to 0.125
- w_gate: bfloat16 [2048, 2048], P('kv', 'tp'), may hold values from -0.125 to 0.125
- lower_bound: float32 [2048], P('tp'), may hold values from 0 to 0.9
- head_gain: float32 [16, 128], P('tp'), may hold values from 0.1 to 1.9
- recur_state: float32 [384, 16, 128, 128], P('kv', 'tp'), may hold values from -3 to 3
- w_out: bfloat16 [2048, 2048], P('tp', 'kv'), may hold values from -0.125 to 0.125
- mixer_gain: float32 [2048], P('kv'), may hold values from 0.1 to 1.9
- w_up: bfloat16 [2048, 8192], P('kv', 'tp'), may hold values from -0.125 to 0.125
- w_down: bfloat16 [8192, 2048], P('tp', 'kv'), may hold values from -0.0625 to 0.0625
Outputs:
- next_tokens: bfloat16 [384, 2048], P('tp', 'kv')
- next_state: float32 [384, 16, 128, 128], P('kv', 'tp')
All inputs are finite; a program needn't handle non-finite values.
Results may differ from a plain program's by a relative error of at most 0.03.
Values may be sent and summed in bfloat16 or wider, within the bound.
A program may use at most 64 MiB of HBM per device.

v0:
```python
import math

import jax
import jax.numpy as jnp
from jax import lax
from jax.sharding import PartitionSpec as P

NORM_EPS = 1e-05


def laid_out(tiles, dim):
    tiles = jnp.moveaxis(tiles, 0, dim)
    dims = tiles.shape
    return tiles.reshape(*dims[:dim], dims[dim] * dims[dim + 1], *dims[dim + 2 :])


def from_everyone(value, axis):
    size = lax.axis_size(axis)
    return lax.all_to_all(
        jnp.broadcast_to(value[None], (size, *value.shape)), axis, 0, 0, tiled=True
    )


def gathered_copies(value, axis, dim):
    return laid_out(from_everyone(value, axis), dim)


def in_blocks(value, dim, size):
    dims = value.shape
    tiles = value.reshape(*dims[:dim], size, dims[dim] // size, *dims[dim + 1 :])
    return jnp.moveaxis(tiles, dim, 0)


def summed_on_arrival(value, axis, dim):
    tiles = in_blocks(value, dim, lax.axis_size(axis))
    arrived = lax.all_to_all(tiles, axis, split_axis=0, concat_axis=0, tiled=True)
    return arrived.astype(jnp.float32).sum(axis=0)


def taken_together(value, axis):
    return from_everyone(value, axis).sum(axis=0)


def in_one_piece(arrays, axis, dim, along):
    widths = [math.prod(a.shape[along:]) for a in arrays]
    both = jnp.concatenate(
        [a.reshape(*a.shape[:along], w) for a, w in zip(arrays, widths)], axis=along
    )
    result = summed_on_arrival(both, axis, dim)
    tiles = jnp.split(result, [sum(widths[:k]) for k in range(1, len(widths))], axis=along)
    return tuple(
        (b.reshape(*result.shape[:along], *a.shape[along:]) for a, b in zip(arrays, tiles))
    )


def project_in(row_block, norm_scale, weights, by_units):
    whole = gathered_copies(row_block, "tp", 0)
    tokens_f = whole.astype(jnp.float32)
    normed = (tokens_f * norm_scale).astype(jnp.bfloat16)
    squares = jnp.sum(tokens_f * tokens_f, axis=1)
    weight = jnp.concatenate(weights, axis=1)
    partial_value = jnp.dot(normed, weight, preferred_element_type=jnp.float32)
    width = normed.shape[1] * lax.axis_size("kv")
    if by_units:
        unit_cols = summed_on_arrival(partial_value.astype(jnp.bfloat16), "kv", 1)
        totals = taken_together(squares, "kv")
        return unit_cols * lax.rsqrt(totals / width + NORM_EPS)[:, None]
    owned, owned_sq = in_one_piece(
        (partial_value.astype(jnp.bfloat16), squares.astype(jnp.bfloat16)), "kv", 0, 1
    )
    row_scale = lax.rsqrt(owned_sq / width + NORM_EPS)
    return owned * row_scale[:, None]


def finish_out(partials):
    return summed_on_arrival(partials.astype(jnp.bfloat16), "tp", 0)


def project_out(values_bf, weight):
    product = jnp.dot(
        gathered_copies(values_bf, "kv", 0), weight, preferred_element_type=jnp.float32
    )
    partials = product.astype(jnp.bfloat16).astype(jnp.float32)
    return finish_out(partials)


def fold_out(values_bf, weight):
    summed = jnp.dot(
        gathered_copies(values_bf, "kv", 1), weight, preferred_element_type=jnp.float32
    )
    return finish_out(summed.astype(jnp.bfloat16).astype(jnp.float32))


def body(
    tokens,
    norm_gain,
    w_query,
    w_forget,
    w_input,
    w_gate,
    lower_bound,
    head_gain,
    recur_state,
    w_out,
    mixer_gain,
    w_up,
    w_down,
):
    projected = project_in(tokens, norm_gain, (w_query, w_forget, w_input, w_gate), False)
    rows_here = projected.shape[0]
    heads_here = recur_state.shape[1]
    key_size = recur_state.shape[2]
    val_size = recur_state.shape[3]
    span = heads_here * key_size
    val_span = heads_here * val_size
    queries = projected[:, :span].reshape(rows_here, heads_here, key_size)
    forget_raw = projected[:, span : 2 * span].reshape(rows_here, heads_here, key_size)
    values_in = projected[:, 2 * span : 2 * span + val_span].reshape(
        rows_here, heads_here, val_size
    )
    gate_raw = projected[:, 2 * span + val_span :]
    bound = lower_bound.reshape(heads_here, key_size)
    forget = bound + (1.0 - bound) * jax.nn.sigmoid(forget_raw)
    next_state = (
        forget[..., None] * recur_state + (1.0 - forget)[..., None] * values_in[:, :, None, :]
    )
    read_out = jnp.einsum("rhk,rhkv->rhv", queries, next_state, precision=lax.Precision.HIGHEST)
    read_out = (
        read_out
        * lax.rsqrt(jnp.mean(read_out * read_out, axis=2, keepdims=True) + NORM_EPS)
        * head_gain
    )
    mixture = (read_out.reshape(rows_here, val_span) * jax.nn.silu(gate_raw)).astype(jnp.bfloat16)
    mixed_rows = (tokens.astype(jnp.float32) + project_out(mixture, w_out)).astype(jnp.bfloat16)
    hidden_pre = project_in(mixed_rows, mixer_gain, (w_up,), True)
    hidden = jnp.square(jax.nn.relu(hidden_pre)).astype(jnp.bfloat16)
    down_out = fold_out(hidden, w_down)
    next_tokens = (mixed_rows.astype(jnp.float32) + down_out).astype(jnp.bfloat16)
    return (next_tokens, next_state)


def solution(mesh):
    in_specs = (
        P("tp", "kv"),
        P("kv"),
        P("kv", "tp"),
        P("kv", "tp"),
        P("kv", "tp"),
        P("kv", "tp"),
        P("tp"),
        P("tp", None),
        P("kv", "tp", None, None),
        P("tp", "kv"),
        P("kv"),
        P("kv", "tp"),
        P("tp", "kv"),
    )
    out_specs = (P("tp", "kv"), P("kv", "tp", None, None))
    return jax.shard_map(body, mesh=mesh, in_specs=in_specs, out_specs=out_specs, check_vma=False)
```

profile of v0, /device:TPU:1, one launch (start us, length us, event | category | flops | bytes accessed | tf_op | source)
XLA Modules:
  0.0 173.9 jit_solution(15843388054404118505)
XLA Ops:
  0.6 0.8 broadcast_in_dim.12
  1.5 10.5 %all_to_all.46 = bf16[8,2,1536]{2,1,0:T(2,128)(2,1)S(1)} all-to-all(bf16[8,2,1536]{2,1,0:T(2,128)(2,1)S(1)} %reshape.139), channel_id=1, replica_groups=mesh['kv'=32,'tp'=8] {'tp'}, dimensions={0} | all-to-all | bytes 98304 | tf_op jit(solution)/shard_map/all_to_all | solution.py:19
  12.1 0.1 reshape.140
  12.2 0.1 multiply_reduce_fusion.1
  12.3 0.7 fusion.1
  13.0 0.2 convert_element_type.114
  13.2 1.1 convolution_convert_fusion.1
  14.4 0.2 concatenate.10
  14.6 1.2 pad_maximum_fusion
  15.7 11.2 %all-to-all-start.1 = ((bf16[32,12,1025]{2,1,0:T(8,128)(2,1)}), bf16[32,12,1025]{2,1,0:T(8,128)(2,1)S(1)}, u32[]{:S(2)}, u32[]{:S(2)}) async-start(bf16[32,12,1025]{2,1,0:T(8,128)(2,1)} %pad_maximum_fusion), calls=%async_computation.1 | async-start | bytes 2359296 | tf_op jit(solution)/shard_map/all_to_all | solution.py:36
  26.9 28.6 %all-to-all-done.1 = bf16[32,12,1025]{2,1,0:T(8,128)(2,1)S(1)} async-done(((bf16[32,12,1025]{2,1,0:T(8,128)(2,1)}), bf16[32,12,1025]{2,1,0:T(8,128)(2,1)S(1)}, u32[]{:S(2)}, u32[]{:S(2)}) %all-to-all-start.1) | async-done | bytes 787232 | tf_op jit(solution)/shard_map/all_to_all | solution.py:36
  55.5 0.2 convert_reduce_fusion
  56.0 1.0 multiply_add_fusion
  57.1 1.4 fusion.16
  58.8 16.9 %all_to_all.47 = bf16[32,12,256]{2,1,0:T(8,128)(2,1)S(1)} all-to-all(bf16[32,12,256]{2,1,0:T(8,128)(2,1)S(1)} %broadcast_in_dim.13), channel_id=1, replica_groups=mesh['kv'=32,'tp'=8] {'kv'}, dimensions={0} | all-to-all | bytes 393216 | tf_op jit(solution)/shard_map/all_to_all | solution.py:19
  75.7 0.2 convolution_convert_fusion.3
  76.0 0.8 reshape.141
  76.8 7.0 %all-to-all-start.3 = ((bf16[8,2,1536]{2,1,0:T(2,128)(2,1)}), bf16[8,2,1536]{2,1,0:T(2,128)(2,1)S(1)}, u32[]{:S(2)}, u32[]{:S(2)}) async-start(bf16[8,2,1536]{2,1,0:T(2,128)(2,1)} %reshape.141), calls=%async_computation.3 | async-start | bytes 98304 | tf_op jit(solution)/shard_map/all_to_all | solution.py:36
  83.9 4.7 %all-to-all-done.3 = bf16[8,2,1536]{2,1,0:T(2,128)(2,1)S(1)} async-done(((bf16[8,2,1536]{2,1,0:T(2,128)(2,1)}), bf16[8,2,1536]{2,1,0:T(2,128)(2,1)S(1)}, u32[]{:S(2)}, u32[]{:S(2)}) %all-to-all-start.3) | async-done | bytes 49184 | tf_op jit(solution)/shard_map/all_to_all | solution.py:36
  89.1 7.9 %all_to_all.48 = bf16[8,2,1536]{2,1,0:T(2,128)(2,1)S(1)} all-to-all(bf16[8,2,1536]{2,1,0:T(2,128)(2,1)S(1)} %reshape.143), channel_id=1, replica_groups=mesh['kv'=32,'tp'=8] {'tp'}, dimensions={0} | all-to-all | bytes 98304 | tf_op jit(solution)/shard_map/all_to_all | solution.py:19
  97.4 0.6 broadcast_in_dim.16
  98.0 3.8 %all-to-all-start.6 = ((f32[32,1,384]{2,1,0:T(1,128)}), f32[32,1,384]{2,1,0:T(1,128)S(1)}, u32[]{:S(2)}, u32[]{:S(2)}) async-start(f32[32,1,384]{2,1,0:T(1,128)} %broadcast_in_dim.16), calls=%async_computation.6 | async-start | bytes 98304 | tf_op jit(solution)/shard_map/all_to_all | solution.py:19
  101.9 0.3 convolution_convert_fusion
  102.2 1.2 copy.55
  103.4 7.3 %all-to-all-done.6 = f32[32,1,384]{2,1,0:T(1,128)S(1)} async-done(((f32[32,1,384]{2,1,0:T(1,128)}), f32[32,1,384]{2,1,0:T(1,128)S(1)}, u32[]{:S(2)}, u32[]{:S(2)}) %all-to-all-start.6) | async-done | bytes 49184 | tf_op jit(solution)/shard_map/all_to_all | solution.py:19
  110.7 3.9 %all-to-all-start.5 = ((bf16[32,384,32]{1,2,0:T(8,128)(2,1)}), bf16[32,384,32]{1,2,0:T(8,128)(2,1)S(1)}, u32[]{:S(2)}, u32[]{:S(2)}) async-start(bf16[32,384,32]{1,2,0:T(8,128)(2,1)} %bitcast.8), calls=%async_computation.5 | async-start | bytes 1572864 | tf_op jit(solution)/shard_map/all_to_all | solution.py:36
  114.7 20.5 %all-to-all-done.5 = bf16[32,384,32]{1,2,0:T(8,128)(2,1)S(1)} async-done(((bf16[32,384,32]{1,2,0:T(8,128)(2,1)}), bf16[32,384,32]{1,2,0:T(8,128)(2,1)S(1)}, u32[]{:S(2)}, u32[]{:S(2)}) %all-to-all-start.5) | async-done | bytes 786464 | tf_op jit(solution)/shard_map/all_to_all | solution.py:36
  135.4 25.8 %all_to_all.49 = bf16[32,384,32]{1,2,0:T(8,128)(2,1)S(1)} all-to-all(bf16[32,384,32]{1,2,0:T(8,128)(2,1)S(1)} %broadcast_in_dim.17), channel_id=1, replica_groups=mesh['kv'=32,'tp'=8] {'kv'}, dimensions={0} | all-to-all | bytes 1572864 | tf_op jit(solution)/shard_map/all_to_all | solution.py:19
  161.2 0.2 convolution_convert_fusion.2
  161.6 0.1 reshape.145
  161.8 11.2 %all_to_all.50 = bf16[8,2,1536]{2,1,0:T(2,128)(2,1)S(1)} all-to-all(bf16[8,2,1536]{2,1,0:T(2,128)(2,1)S(1)} %reshape.145), channel_id=1, replica_groups=mesh['kv'=32,'tp'=8] {'tp'}, dimensions={0} | all-to-all | bytes 98304 | tf_op jit(solution)/shard_map/all_to_all | solution.py:36
  173.2 0.7 copy.59
  (58 shorter events, 2.4 us)
Async XLA Ops:
  0.6 101.2 %copy-start = (bf16[64,1024]{1,0:T(8,128)(2,1)S(1)}, bf16[64,1024]{1,0:T(8,128)(2,1)}, u32[]{:S(2)}) copy-start(bf16[64,1024]{1,0:T(8,128)(2,1)} %param.24) | copy-start | bytes 393220
  15.7 11.2 %copy-start.6 = (f32[256]{0:T(256)S(1)}, f32[256]{0:T(256)}, u32[]{:S(2)}) copy-start(f32[256]{0:T(256)} %param.19) | copy-start | bytes 3076
  15.7 40.3 %copy-start.2 = (f32[12,2,128,128]{3,2,1,0:T(8,128)S(1)}, f32[12,2,128,128]{3,2,1,0:T(8,128)}, u32[]{:S(2)}) copy-start(f32[12,2,128,128]{3,2,1,0:T(8,128)} %param.21) | copy-start | bytes 4718596
  15.7 39.8 %all-to-all-start.1 = ((bf16[32,12,1025]{2,1,0:T(8,128)(2,1)}), bf16[32,12,1025]{2,1,0:T(8,128)(2,1)S(1)}, u32[]{:S(2)}, u32[]{:S(2)}) async-start(bf16[32,12,1025]{2,1,0:T(8,128)(2,1)} %pad_maximum_fusion), calls=%async_computation.1 | async-start | bytes 2359296 | tf_op jit(solution)/shard_map/all_to_all | solution.py:36
  57.0 18.9 %copy-start.1 = (f32[12,2,128,128]{3,2,1,0:T(8,128)}, f32[12,2,128,128]{3,2,1,0:T(8,128)S(1)}, u32[]{:S(2)}) copy-start(f32[12,2,128,128]{3,2,1,0:T(8,128)S(1)} %multiply_add_fusion) | copy-start | bytes 4718596
  57.0 1.6 copy-start.7
  57.0 18.6 %copy-start.5 = (bf16[256,64]{0,1:T(8,128)(2,1)S(1)}, bf16[256,64]{0,1:T(8,128)(2,1)}, u32[]{:S(2)}) copy-start(bf16[256,64]{0,1:T(8,128)(2,1)} %param.22) | copy-start | bytes 98308
  57.1 26.7 %copy-start.4 = (bf16[48,64]{1,0:T(8,128)(2,1)S(1)}, bf16[48,64]{1,0:T(8,128)(2,1)}, u32[]{:S(2)}) copy-start(bf16[48,64]{1,0:T(8,128)(2,1)} %param.13) | copy-start | bytes 18436
  58.6 38.8 %copy-start.8 = (f32[64]{0:T(128)S(1)}, f32[64]{0:T(128)}, u32[]{:S(2)}) copy-start(f32[64]{0:T(128)} %param.23) | copy-start | bytes 772
  76.8 11.8 %all-to-all-start.3 = ((bf16[8,2,1536]{2,1,0:T(2,128)(2,1)}), bf16[8,2,1536]{2,1,0:T(2,128)(2,1)S(1)}, u32[]{:S(2)}, u32[]{:S(2)}) async-start(bf16[8,2,1536]{2,1,0:T(2,128)(2,1)} %reshape.141), calls=%async_computation.3 | async-start | bytes 98304 | tf_op jit(solution)/shard_map/all_to_all | solution.py:36
  98.0 12.7 %all-to-all-start.6 = ((f32[32,1,384]{2,1,0:T(1,128)}), f32[32,1,384]{2,1,0:T(1,128)S(1)}, u32[]{:S(2)}, u32[]{:S(2)}) async-start(f32[32,1,384]{2,1,0:T(1,128)} %broadcast_in_dim.16), calls=%async_computation.6 | async-start | bytes 98304 | tf_op jit(solution)/shard_map/all_to_all | solution.py:19
  110.7 24.5 %all-to-all-start.5 = ((bf16[32,384,32]{1,2,0:T(8,128)(2,1)}), bf16[32,384,32]{1,2,0:T(8,128)(2,1)S(1)}, u32[]{:S(2)}, u32[]{:S(2)}) async-start(bf16[32,384,32]{1,2,0:T(8,128)(2,1)} %bitcast.8), calls=%async_computation.5 | async-start | bytes 1572864 | tf_op jit(solution)/shard_map/all_to_all | solution.py:36
  114.7 46.5 %copy-start.3 = (bf16[1024,64]{0,1:T(8,128)(2,1)S(1)}, bf16[1024,64]{0,1:T(8,128)(2,1)}, u32[]{:S(2)}) copy-start(bf16[1024,64]{0,1:T(8,128)(2,1)} %param.25) | copy-start | bytes 393220
where the time goes:
time: 175 us; the launch traced here: 174 us
  blocking collectives  72.4 us (41%)
  waiting for transfers between devices  61.1 us (35%)
  starting transfers between devices  25.9 us (15%)
  local copies, waits for them, and re-layouts  6.19 us (4%)
  other arithmetic  4.01 us (2%)
  matrix products  3.34 us (2%)
    all_to_all x4, blocking collectives, from_everyone(): lax.all_to_all(jnp.broadcast_to(value[None], (size, *value.shape)), axis,...  61.1 us
    all_to_all x3, waiting for transfers between devices, summed_on_arrival(): lax.all_to_all(tiles, axis, split_axis=0, concat_axis=0, tiled=True)  53.8 us
    all_to_all x3, starting transfers between devices, summed_on_arrival(): lax.all_to_all(tiles, axis, split_axis=0, concat_axis=0, tiled=True)  22.1 us
    all_to_all x1, blocking collectives, summed_on_arrival(): lax.all_to_all(tiles, axis, split_axis=0, concat_axis=0, tiled=True)  11.2 us
    all_to_all x1, waiting for transfers between devices, from_everyone(): lax.all_to_all(jnp.broadcast_to(value[None], (size, *value.shape)), axis,...  7.32 us
    all_to_all x1, starting transfers between devices, from_everyone(): lax.all_to_all(jnp.broadcast_to(value[None], (size, *value.shape)), axis,...  3.84 us
  transfers between devices with their start and end apart: 4, of which 4 were waited for; matrix products, arithmetic and copies ran while one was open for 1% of the time, Pallas kernels for 0%

commit v1 on v0

v1 whole, which is shorter than its diff:
```python
import functools

import jax
import jax.numpy as jnp
from jax import lax
from jax.experimental import pallas as pl
from jax.experimental.pallas import tpu as pltpu
from jax.sharding import PartitionSpec as P

NORM_EPS = 1e-05
MESH = pl.DeviceIdType.MESH
F32 = jnp.float32
BF16 = jnp.bfloat16

NZ, NX, NT = 8, 4, 8
WIDTH = 2048.0


def far_first(step, size):
    return ((step + 1) // 2) * (1 - 2 * (step % 2)) + size // 2


def wait_for(ref, sem):
    pltpu.make_async_copy(ref, ref, sem).wait()


def swap_lanes(value):
    return pltpu.roll(value, 64, 1)


def dot_t(a, b):
    return lax.dot_general(a, b, (((1,), (1,)), ((), ())), preferred_element_type=F32)


def low_lanes(shape):
    return lax.broadcasted_iota(jnp.int32, shape, 1) < 64


def unpacked(pieces):
    low = low_lanes(pieces[0].shape)
    swapped = [swap_lanes(p) for p in pieces]
    first = [jnp.where(low, pieces[i], swapped[i + 1]).astype(BF16) for i in (0, 2)]
    second = [jnp.where(low, swapped[i], pieces[i + 1]).astype(BF16) for i in (0, 2)]
    return jnp.concatenate(
        [jnp.concatenate(first, axis=1), jnp.concatenate(second, axis=1)], axis=0
    )


def row_squares(pieces):
    total = pieces[0] * pieces[0]
    for p in pieces[1:]:
        total = total + p * p
    total = jnp.concatenate([total, jnp.zeros((64, 128), F32)], axis=0)
    high = total.astype(BF16)
    rest = (total - high.astype(F32)).astype(BF16)
    lane = lax.broadcasted_iota(jnp.int32, (8, 128), 1)
    row = lax.broadcasted_iota(jnp.int32, (8, 128), 0)
    pick = jnp.where((lane // 64) == row, 1.0, 0.0).astype(BF16)
    dims = (((1,), (1,)), ((), ()))
    sums = lax.dot_general(pick, high, dims, preferred_element_type=F32)
    sums = sums + lax.dot_general(pick, rest, dims, preferred_element_type=F32)
    return sums[0:2, :]


def column_of(values, base, period):
    lane = lax.broadcasted_iota(jnp.int32, (24, 256), 1)
    row = lax.broadcasted_iota(jnp.int32, (24, 256), 0)
    return jnp.sum(
        jnp.where(lane == base + row % period, values, 0.0), axis=1, keepdims=True
    )


def kernel(
    tokens_hbm,
    gains_hbm,
    wq_hbm,
    wf_hbm,
    wi_hbm,
    wg_hbm,
    bound_hbm,
    head_gain_hbm,
    state_hbm,
    wout_hbm,
    wup_hbm,
    wdown_hbm,
    out_ref,
    next_hbm,
    tok_v,
    gain_v,
    w4_v,
    bound_v,
    head_gain_v,
    state_v,
    next_v,
    wout_v,
    wup_v,
    wdown_v,
    gains,
    w_first,
    w_up,
    w_down,
    w_out,
    tok_all,
    sq1,
    proj_out,
    proj_in,
    mix_own,
    mix_all,
    mixed_all,
    sq2,
    up_out,
    up_in,
    hidden_all,
    down_out,
    down_in,
    read_v,
    in_sems,
    send_sems,
    recv_sems,
):
    kv, t = lax.axis_index("kv"), lax.axis_index("tp")
    z, x = kv // NX, kv % NX
    y, core = t // 2, t % 2
    rows_at = (t + NZ - z) % NZ
    has_self = t == (2 * z) % NZ

    def in_plane(i):
        px = (x + far_first(i // 8, 4)) % 4
        py = (y + far_first((i % 8) // 2, 4)) % 4
        pc = (core + 1 - i % 2) % 2
        return px, 2 * py + pc

    def in_column(i):
        pz = (z + far_first(i // 4, 8)) % 8
        px = (x + far_first(i % 4, 4)) % 4
        return pz, px

    def copy_to(src, dst, k, pkv, pt):
        return pltpu.make_async_remote_copy(
            src_ref=src,
            dst_ref=dst,
            send_sem=send_sems.at[k],
            recv_sem=recv_sems.at[k],
            device_id=(pkv, pt),
            device_id_type=MESH,
        )

    barrier = pltpu.get_barrier_semaphore()

    def tell(pkv, pt):
        pl.semaphore_signal(barrier, inc=1, device_id=(pkv, pt), device_id_type=MESH)

    def greet_plane(i, c):
        px, pt = in_plane(i)
        tell(z * NX + px, pt)
        return c

    def greet_column(i, c):
        pz, px = in_column(i)
        tell(pz * NX + px, t)
        return c

    lax.fori_loop(0, 31, greet_column, 0)

    def greet_mix(i, c):
        skv, st = rows_at * NX + i // 8, i % 8

        @pl.when(jnp.logical_or(skv != kv, st != t))
        def _():
            tell(skv, st)

        return c

    lax.fori_loop(0, 32, greet_mix, 0)
    lax.fori_loop(0, 31, greet_plane, 0)

    loads = [
        pltpu.make_async_copy(tokens_hbm, tok_v, in_sems.at[0]),
        pltpu.make_async_copy(gains_hbm, gain_v, in_sems.at[1]),
        pltpu.make_async_copy(wq_hbm, w4_v.at[0], in_sems.at[2]),
        pltpu.make_async_copy(wf_hbm, w4_v.at[1], in_sems.at[3]),
        pltpu.make_async_copy(wi_hbm, w4_v.at[2], in_sems.at[4]),
        pltpu.make_async_copy(wg_hbm, w4_v.at[3], in_sems.at[5]),
        pltpu.make_async_copy(wout_hbm, wout_v, in_sems.at[6]),
        pltpu.make_async_copy(wup_hbm, wup_v, in_sems.at[7]),
        pltpu.make_async_copy(wdown_hbm, wdown_v, in_sems.at[8]),
        pltpu.make_async_copy(bound_hbm, bound_v, in_sems.at[9]),
        pltpu.make_async_copy(head_gain_hbm, head_gain_v, in_sems.at[10]),
        pltpu.make_async_copy(state_hbm, state_v, in_sems.at[11]),
    ]
    for load in loads:
        load.start()

    loads[0].wait()
    tok_f = tok_v[...].astype(F32)
    tok_all[x * NT + t] = jnp.concatenate([tok_f[0:24], tok_f[24:48]], axis=1).astype(BF16)
    loads[1].wait()
    g = gain_v[...]
    gains[x] = jnp.concatenate([g, g], axis=1)
    for k in range(2, 9):
        loads[k].wait()
    w_first[x] = w4_v[x]
    w_up[x] = wup_v[:, pl.ds(pl.multiple_of(x * 256, 256), 256)]
    w_out[t] = wout_v[...]
    w_down[x] = wdown_v[:, pl.ds(pl.multiple_of(x * 256, 256), 256)]

    pl.semaphore_wait(barrier, 31 + 31 + 32 - has_self.astype(jnp.int32))

    def send_tokens(i, c):
        px, pt = in_plane(i)
        copy_to(tok_all.at[x * NT + t], tok_all.at[x * NT + t], 0, z * NX + px, pt).start()
        return c

    def send_first(i, c):
        px = (x + far_first(i, 4)) % 4
        copy_to(gains.at[x], gains.at[x], 1, z * NX + px, t).start()
        copy_to(w4_v.at[px], w_first.at[x], 2, z * NX + px, t).start()
        return c

    lax.fori_loop(0, 3, send_first, 0)
    lax.fori_loop(0, 31, send_tokens, 0)

    wait_for(gains.at[pl.ds(0, 3)], recv_sems.at[1])
    wait_for(tok_all.at[pl.ds(0, 31)], recv_sems.at[0])

    def send_wout(i, c):
        py = (y + far_first(i // 2, 4)) % 4
        pt = 2 * py + (core + 1 - i % 2) % 2
        copy_to(w_out.at[t], w_out.at[t], 3, kv, pt).start()
        return c

    lax.fori_loop(0, 7, send_wout, 0)

    raw = [
        tok_all[pl.ds(NT * q, NT)].astype(F32).reshape(192, 128) for q in range(NX)
    ]
    sq1[z] = row_squares(raw)
    lhs = unpacked([raw[q] * gains[q, 0:1, :] for q in range(NX)])
    wait_for(w_first.at[pl.ds(0, 3)], recv_sems.at[2])
    partial = jnp.dot(lhs, w_first[...].reshape(256, 256), preferred_element_type=F32)

    for half in range(2):
        for pz in range(NZ):
            at = half * 192 + pz * 24
            left = partial[at : at + 24, 0:128]
            right = partial[at : at + 24, 128:256]
            proj_out[pz * NX + 2 * half] = jnp.concatenate(
                [left[0:12], right[0:12]], axis=0
            ).astype(BF16)
            proj_out[pz * NX + 2 * half + 1] = jnp.concatenate(
                [left[12:24], right[12:24]], axis=0
            ).astype(BF16)

    def send_sq1(i, c):
        pz = (z + far_first(i, 8)) % 8
        copy_to(sq1.at[z], sq1.at[z], 4, pz * NX + x, t).start()
        return c

    def send_proj(i, c):
        pz, px = in_column(i)
        copy_to(proj_out.at[pz * NX + px], proj_in.at[kv], 5, pz * NX + px, t).start()
        return c

    lax.fori_loop(0, 7, send_sq1, 0)
    lax.fori_loop(0, 31, send_proj, 0)
    proj_in[kv] = proj_out[kv]

    def send_ffn(i, c):
        px = (x + far_first(i, 4)) % 4
        cols = pl.ds(pl.multiple_of(px * 256, 256), 256)
        copy_to(wup_v.at[:, cols], w_up.at[x], 6, z * NX + px, t).start()
        copy_to(wdown_v.at[:, cols], w_down.at[x], 7, z * NX + px, t).start()
        return c

    lax.fori_loop(0, 3, send_ffn, 0)

    for k in range(9, 12):
        loads[k].wait()
    wait_for(sq1.at[pl.ds(0, 7)], recv_sems.at[4])
    wait_for(proj_in.at[pl.ds(0, 31)], recv_sems.at[5])

    squares = sq1[0]
    for q in range(1, NZ):
        squares = squares + sq1[q]
    square_row = jnp.where(x // 2 == 0, squares[0:1, :], squares[1:2, :])
    row_scale = lax.rsqrt(
        column_of(square_row, z * 24 + (x % 2) * 12, 12) / WIDTH + NORM_EPS
    )
    owned = []
    for q in range(NX):
        total = proj_in[q].astype(F32)
        for r in range(1, NZ):
            total = total + proj_in[r * NX + q].astype(F32)
        owned.append(total * row_scale)
    queries, forget_raw, values_in, gate_raw = owned
    head0 = lax.broadcasted_iota(jnp.int32, (24, 128), 0) < 12
    bound = jnp.where(head0, bound_v[0:1, :], bound_v[1:2, :])
    head_gain = jnp.where(head0, head_gain_v[0:1, :], head_gain_v[1:2, :])
    forget = bound + (1.0 - bound) * jax.nn.sigmoid(forget_raw)
    pad = jnp.zeros((104, 128), F32)
    forget_t = jnp.concatenate([forget, pad], axis=0).T
    queries_t = jnp.concatenate([queries, pad], axis=0).T
    for j in range(24):
        h, s = j // 12, j % 12
        f = forget_t[:, j : j + 1]
        nxt = f * state_v[s, h] + (1.0 - f) * values_in[j : j + 1, :]
        next_v[s, h] = nxt
        read_v[j : j + 1, :] = jnp.sum(queries_t[:, j : j + 1] * nxt, axis=0, keepdims=True)
    store = pltpu.make_async_copy(next_v, next_hbm, in_sems.at[12])
    store.start()
    read = read_v[...]
    read = read * lax.rsqrt(jnp.mean(read * read, axis=1, keepdims=True) + NORM_EPS) * head_gain
    mix_own[...] = (read * jax.nn.silu(gate_raw)).astype(BF16)

    def send_mix(i, c):
        pz, px = (z + far_first(i // 4, 8)) % 8, (x + far_first(i % 4, 4)) % 4
        pt = (z + pz) % NZ
        away = jnp.logical_or(pz * NX + px != kv, pt != t)

        @pl.when(away)
        def _():
            copy_to(mix_own, mix_all.at[t * NX + x], 8, pz * NX + px, pt).start()

        return c

    lax.fori_loop(0, 32, send_mix, 0)

    @pl.when(has_self)
    def _():
        mix_all[t * NX + x] = mix_own[...]

    wait_for(w_out.at[pl.ds(0, 7)], recv_sems.at[3])

    @pl.when(has_self)
    def _():
        wait_for(mix_all.at[pl.ds(0, 31)], recv_sems.at[8])

    @pl.when(jnp.logical_not(has_self))
    def _():
        wait_for(mix_all, recv_sems.at[8])

    acc = jnp.zeros((96, 128), F32)
    for q in range(NT):
        both = jnp.concatenate([w_out[q, :, 0:128], w_out[q, :, 128:256]], axis=0)
        acc = acc + dot_t(mix_all[4 * q : 4 * q + 4].reshape(96, 128), both)
    folded = []
    for q in range(NX):
        part = acc[24 * q : 24 * q + 24]
        turned = swap_lanes(jnp.concatenate([part[12:24], part[0:12]], axis=0))
        folded.append(part + turned)
    low = low_lanes((24, 128))
    top = jnp.where(low, folded[0], swap_lanes(folded[2]))
    bottom = jnp.where(low, swap_lanes(folded[1]), folded[3])
    attn = jnp.where(head0, top, bottom)
    own_at = x * NT + rows_at
    mixed_all[own_at] = (tok_all[own_at].astype(F32) + attn).astype(BF16)

    def send_mixed(i, c):
        px, pt = in_plane(i)
        copy_to(mixed_all.at[own_at], mixed_all.at[own_at], 9, z * NX + px, pt).start()
        return c

    lax.fori_loop(0, 31, send_mixed, 0)
    wait_for(w_up.at[pl.ds(0, 3)], recv_sems.at[6])
    wait_for(mixed_all.at[pl.ds(0, 31)], recv_sems.at[9])

    raw2 = [
        mixed_all[pl.ds(NT * q, NT)].astype(F32).reshape(192, 128) for q in range(NX)
    ]
    sq2[z] = row_squares(raw2)
    lhs2 = unpacked([raw2[q] * gains[q, 1:2, :] for q in range(NX)])
    partial2 = jnp.dot(lhs2, w_up[...].reshape(256, 256), preferred_element_type=F32)
    for half in range(2):
        for pz in range(NZ):
            at = half * 192 + pz * 24
            up_out[pz, half] = partial2[at : at + 24].astype(BF16)

    def send_up(i, c):
        pz = (z + far_first(i, 8)) % 8
        copy_to(sq2.at[z], sq2.at[z], 10, pz * NX + x, t).start()
        copy_to(up_out.at[pz], up_in.at[z], 11, pz * NX + x, t).start()
        return c

    lax.fori_loop(0, 7, send_up, 0)
    up_in[z] = up_out[z]
    wait_for(sq2.at[pl.ds(0, 7)], recv_sems.at[10])
    squares2 = sq2[0]
    for q in range(1, NZ):
        squares2 = squares2 + sq2[q]
    scales = [
        lax.rsqrt(column_of(squares2[q : q + 1, :], z * 24, 24) / WIDTH + NORM_EPS)
        for q in range(2)
    ]
    wait_for(up_in.at[pl.ds(0, 7)], recv_sems.at[11])

    for half in range(2):
        total = up_in[0, half].astype(F32)
        for q in range(1, NZ):
            total = total + up_in[q, half].astype(F32)
        total = jnp.maximum(total * scales[half], 0.0)
        hidden_all[z, half] = (total * total).astype(BF16)

    def send_hidden(i, c):
        pz = (z + far_first(i, 8)) % 8
        copy_to(hidden_all.at[z], hidden_all.at[z], 12, pz * NX + x, t).start()
        return c

    lax.fori_loop(0, 7, send_hidden, 0)
    wait_for(w_down.at[pl.ds(0, 3)], recv_sems.at[7])
    wait_for(hidden_all.at[pl.ds(0, 7)], recv_sems.at[12])

    partial3 = dot_t(hidden_all[...].reshape(384, 256), w_down[...].reshape(256, 256))
    for pt in range(NT):
        for pair in range(2):
            upper = partial3[48 * pt : 48 * pt + 24, 128 * pair : 128 * pair + 128]
            lower = partial3[48 * pt + 24 : 48 * pt + 48, 128 * pair : 128 * pair + 128]
            down_out[pt * NX + 2 * pair] = jnp.where(low, upper, swap_lanes(lower)).astype(BF16)
            down_out[pt * NX + 2 * pair + 1] = jnp.where(low, swap_lanes(upper), lower).astype(
                BF16
            )

    def send_down(i, c):
        px, pt = in_plane(i)
        copy_to(
            down_out.at[pt * NX + px], down_in.at[t * NX + x], 13, z * NX + px, pt
        ).start()
        return c

    lax.fori_loop(0, 31, send_down, 0)
    down_in[t * NX + x] = down_out[t * NX + x]
    wait_for(down_in.at[pl.ds(0, 31)], recv_sems.at[13])
    total = down_in[0].astype(F32)
    for q in range(1, 32):
        total = total + down_in[q].astype(F32)
    total = mixed_all[x * NT + t].astype(F32) + total
    out_ref[...] = jnp.concatenate([total[:, 0:64], total[:, 64:128]], axis=0).astype(BF16)

    store.wait()
    wait_for(tok_all.at[pl.ds(0, 31)], send_sems.at[0])
    wait_for(gains.at[pl.ds(0, 3)], send_sems.at[1])
    wait_for(w_first.at[pl.ds(0, 3)], send_sems.at[2])
    wait_for(w_out.at[pl.ds(0, 7)], send_sems.at[3])
    wait_for(sq1.at[pl.ds(0, 7)], send_sems.at[4])
    wait_for(proj_in.at[pl.ds(0, 31)], send_sems.at[5])
    wait_for(w_up.at[pl.ds(0, 3)], send_sems.at[6])
    wait_for(w_down.at[pl.ds(0, 3)], send_sems.at[7])

    @pl.when(has_self)
    def _():
        wait_for(mix_all.at[pl.ds(0, 31)], send_sems.at[8])

    @pl.when(jnp.logical_not(has_self))
    def _():
        wait_for(mix_all, send_sems.at[8])

    wait_for(mixed_all.at[pl.ds(0, 31)], send_sems.at[9])
    wait_for(sq2.at[pl.ds(0, 7)], send_sems.at[10])
    wait_for(up_in.at[pl.ds(0, 7)], send_sems.at[11])
    wait_for(hidden_all.at[pl.ds(0, 7)], send_sems.at[12])
    wait_for(down_in.at[pl.ds(0, 31)], send_sems.at[13])


def body(
    tokens,
    norm_gain,
    w_query,
    w_forget,
    w_input,
    w_gate,
    lower_bound,
    head_gain,
    recur_state,
    w_out,
    mixer_gain,
    w_up,
    w_down,
):
    gains = jnp.stack([norm_gain, mixer_gain])
    bound = lower_bound.reshape(2, 128)
    any_spec = pl.BlockSpec(memory_space=pl.ANY)
    return pl.pallas_call(
        kernel,
        out_shape=(
            jax.ShapeDtypeStruct(tokens.shape, tokens.dtype),
            jax.ShapeDtypeStruct(recur_state.shape, recur_state.dtype),
        ),
        in_specs=[any_spec] * 12,
        out_specs=(pl.BlockSpec(memory_space=pltpu.VMEM), any_spec),
        scratch_shapes=[
            pltpu.VMEM((48, 64), BF16),
            pltpu.VMEM((2, 64), F32),
            pltpu.VMEM((4, 64, 256), BF16),
            pltpu.VMEM((2, 128), F32),
            pltpu.VMEM((2, 128), F32),
            pltpu.VMEM((12, 2, 128, 128), F32),
            pltpu.VMEM((12, 2, 128, 128), F32),
            pltpu.VMEM((64, 256), BF16),
            pltpu.VMEM((64, 1024), BF16),
            pltpu.VMEM((64, 1024), BF16),
            pltpu.VMEM((4, 2, 128), F32),
            pltpu.VMEM((4, 64, 256), BF16),
            pltpu.VMEM((4, 64, 256), BF16),
            pltpu.VMEM((4, 64, 256), BF16),
            pltpu.VMEM((8, 64, 256), BF16),
            pltpu.VMEM((32, 24, 128), BF16),
            pltpu.VMEM((8, 2, 256), F32),
            pltpu.VMEM((32, 24, 128), BF16),
            pltpu.VMEM((32, 24, 128), BF16),
            pltpu.VMEM((24, 128), BF16),
            pltpu.VMEM((32, 24, 128), BF16),
            pltpu.VMEM((32, 24, 128), BF16),
            pltpu.VMEM((8, 2, 256), F32),
            pltpu.VMEM((8, 2, 24, 256), BF16),
            pltpu.VMEM((8, 2, 24, 256), BF16),
            pltpu.VMEM((8, 2, 24, 256), BF16),
            pltpu.VMEM((32, 24, 128), BF16),
            pltpu.VMEM((32, 24, 128), BF16),
            pltpu.VMEM((24, 128), F32),
            pltpu.SemaphoreType.DMA((13,)),
            pltpu.SemaphoreType.DMA((14,)),
            pltpu.SemaphoreType.DMA((14,)),
        ],
        compiler_params=pltpu.CompilerParams(collective_id=0, has_side_effects=True),
        name="decode_layer",
    )(
        tokens,
        gains,
        w_query,
        w_forget,
        w_input,
        w_gate,
        bound,
        head_gain,
        recur_state,
        w_out.T,
        w_up,
        w_down.T,
    )


def solution(mesh):
    in_specs = (
        P("tp", "kv"),
        P("kv"),
        P("kv", "tp"),
        P("kv", "tp"),
        P("kv", "tp"),
        P("kv", "tp"),
        P("tp"),
        P("tp", None),
        P("kv", "tp", None, None),
        P("tp", "kv"),
        P("kv"),
        P("kv", "tp"),
        P("tp", "kv"),
    )
    out_specs = (P("tp", "kv"), P("kv", "tp", None, None))
    return jax.shard_map(body, mesh=mesh, in_specs=in_specs, out_specs=out_specs, check_vma=False)
```

time: 175 us -> 71.4 us (0.41)
  blocking collectives: 72.4 us -> 0 us
  Pallas kernels: 0 us -> 65.2 us
  waiting for transfers between devices: 61.1 us -> 0 us
  starting transfers between devices: 25.9 us -> 0 us
  matrix products: 3.34 us -> 0 us
  other arithmetic: 4.01 us -> 1.24 us
  local copies, waits for them, and re-layouts: 6.19 us -> 4.01 us
    all_to_all x5 -> x0, blocking collectives: 72.4 us -> none  [the longest x4 61.1 us: from_everyone(): lax.all_to_all(jnp.broadcast_to(value[None], (size, *value.shape)), axis,...]
    pallas_call x0 -> x1, Pallas kernels: none -> 65.2 us  [body(): pl.pallas_call(kernel, out_shape=(jax.ShapeDtypeStruct(tokens.shape, toke...]
    all_to_all x4 -> x0, waiting for transfers between devices: 61.1 us -> none  [the longest x3 53.8 us: summed_on_arrival(): lax.all_to_all(tiles, axis, split_axis=0, concat_axis=0, tiled=True)]
    all_to_all x4 -> x0, starting transfers between devices: 25.9 us -> none  [the longest x3 22.1 us: summed_on_arrival(): lax.all_to_all(tiles, axis, split_axis=0, concat_axis=0, tiled=True)]
    dot_general x5 -> x0, matrix products: 3.34 us -> none  [the longest x2 1.48 us: project_in(): partial_value = jnp.dot(normed, weight, preferred_element_type=jnp.float32)]
    unnamed x32 -> x2, local copies, waits for them, and re-layouts: 2.64 us -> 4.01 us
  transfers between devices with their start and end apart: 4 -> 0, of which waited for: 4 -> 0; matrix products, arithmetic and copies ran while one was open for 1% -> 0% of each run, Pallas kernels for 0% -> 0%
where the time goes in v1:
time: 71.4 us; the launch traced here: 71.1 us
  Pallas kernels  65.2 us (91%)
  local copies, waits for them, and re-layouts  4.01 us (6%)
  other arithmetic  1.24 us (2%)
    pallas_call x1, Pallas kernels, body(): pl.pallas_call(kernel, out_shape=(jax.ShapeDtypeStruct(tokens.shape, toke...  65.2 us
    unnamed x2, local copies, waits for them, and re-layouts  4.01 us

profile of v1, /device:TPU:1, one launch (start us, length us, event | category | flops | bytes accessed | tf_op | source)
XLA Modules:
  0.0 71.1 jit_solution(11727518619458547810)
XLA Ops:
  0.6 1.2 %pad_maximum_fusion.gains_hbm = f32[2,64]{1,0:T(2,128)} fusion(f32[1,64]{1,0:T(1,128)} %bitcast.8, f32[1,64]{1,0:T(1,128)} %bitcast.9), kind=kLoop, calls=%fused_computation | loop fusion | flops 128 | bytes 1024 | tf_op jit(solution)/shard_map/stack | solution.py:478
  1.9 65.2 %decode_layer.1 = (bf16[48,64]{1,0:T(8,128)(2,1)}, f32[12,2,128,128]{3,2,1,0:T(8,128)}) custom-call(bf16[48,64]{1,0:T(8,128)(2,1)} %tokens_hbm.1, f32[2,64]{1,0:T(2,128)} %pad_maximum_fusion.gains_hbm, bf16[64,256]{1,0:T(8,128)(2,1)} %wq_hbm.1, bf16[64,256]{1,0:T(8,128)(2,1)} %wf_hbm.1, bf16[64,256]{1,0:T(8,128)(2,1)} %wi_hbm.1, bf16[64,256]{1,0:T(8,128)(2,1)} %wg_hbm.1, ...), custom_call_target="tpu_custom_call" | custom-call | tf_op jit(solution)/shard_map/decode_layer/pallas_call | solution.py:481
  67.1 1.3 %copy.17 = bf16[48,64]{1,0:T(8,128)(2,1)} copy(bf16[48,64]{1,0:T(8,128)(2,1)} %get-tuple-element.4) | data formatting | bytes 12288
  68.4 2.7 %copy.18 = f32[12,2,128,128]{3,2,1,0:T(8,128)} copy(f32[12,2,128,128]{3,2,1,0:T(8,128)} %get-tuple-element.5) | data formatting | bytes 3145728

commit v2 on v1

--- a/solution.py
+++ b/solution.py
@@ -72,7 +72,8 @@
 
 def kernel(
     tokens_hbm,
-    gains_hbm,
+    norm_gain_hbm,
+    mixer_gain_hbm,
     wq_hbm,
     wf_hbm,
     wi_hbm,
@@ -84,14 +85,13 @@
     wup_hbm,
     wdown_hbm,
     out_ref,
-    next_hbm,
+    next_v,
     tok_v,
     gain_v,
     w4_v,
     bound_v,
     head_gain_v,
     state_v,
-    next_v,
     wout_v,
     wup_v,
     wdown_v,
@@ -117,6 +117,7 @@
     in_sems,
     send_sems,
     recv_sems,
+    far_sem,
 ):
     kv, t = lax.axis_index("kv"), lax.axis_index("tp")
     z, x = kv // NX, kv % NX
@@ -145,6 +146,20 @@
             device_id_type=MESH,
         )
 
+    leaving, mix_sent = [], []
+
+    def finish():
+        for ref, k in leaving:
+            wait_for(ref, send_sems.at[k])
+        if mix_sent:
+            @pl.when(has_self)
+            def _():
+                wait_for(mix_all.at[pl.ds(0, 31)], send_sems.at[8])
+
+            @pl.when(jnp.logical_not(has_self))
+            def _():
+                wait_for(mix_all, send_sems.at[8])
+
     barrier = pltpu.get_barrier_semaphore()
 
     def tell(pkv, pt):
@@ -155,28 +170,17 @@
         tell(z * NX + px, pt)
         return c
 
-    def greet_column(i, c):
-        pz, px = in_column(i)
-        tell(pz * NX + px, t)
-        return c
-
-    lax.fori_loop(0, 31, greet_column, 0)
-
-    def greet_mix(i, c):
-        skv, st = rows_at * NX + i // 8, i % 8
-
-        @pl.when(jnp.logical_or(skv != kv, st != t))
-        def _():
-            tell(skv, st)
-
-        return c
-
-    lax.fori_loop(0, 32, greet_mix, 0)
+    def greet_near(i, c):
+        pz = (z + (i // 8 + 1) * (1 - 2 * ((i // 4) % 2)) + NZ) % NZ
+        tell(pz * NX + (x + i) % NX, t)
+        return c
+
     lax.fori_loop(0, 31, greet_plane, 0)
+    lax.fori_loop(0, 16, greet_near, 0)
 
     loads = [
         pltpu.make_async_copy(tokens_hbm, tok_v, in_sems.at[0]),
-        pltpu.make_async_copy(gains_hbm, gain_v, in_sems.at[1]),
+        pltpu.make_async_copy(norm_gain_hbm, gain_v.at[0], in_sems.at[1]),
         pltpu.make_async_copy(wq_hbm, w4_v.at[0], in_sems.at[2]),
         pltpu.make_async_copy(wf_hbm, w4_v.at[1], in_sems.at[3]),
         pltpu.make_async_copy(wi_hbm, w4_v.at[2], in_sems.at[4]),
@@ -187,6 +191,7 @@
         pltpu.make_async_copy(bound_hbm, bound_v, in_sems.at[9]),
         pltpu.make_async_copy(head_gain_hbm, head_gain_v, in_sems.at[10]),
         pltpu.make_async_copy(state_hbm, state_v, in_sems.at[11]),
+        pltpu.make_async_copy(mixer_gain_hbm, gain_v.at[1], in_sems.at[12]),
     ]
     for load in loads:
         load.start()
@@ -195,8 +200,10 @@
     tok_f = tok_v[...].astype(F32)
     tok_all[x * NT + t] = jnp.concatenate([tok_f[0:24], tok_f[24:48]], axis=1).astype(BF16)
     loads[1].wait()
-    g = gain_v[...]
-    gains[x] = jnp.concatenate([g, g], axis=1)
+    loads[12].wait()
+    for q in range(2):
+        g = gain_v[q]
+        gains[x, q : q + 1, :] = jnp.concatenate([g, g], axis=1)
     for k in range(2, 9):
         loads[k].wait()
     w_first[x] = w4_v[x]
@@ -204,7 +211,11 @@
     w_out[t] = wout_v[...]
     w_down[x] = wdown_v[:, pl.ds(pl.multiple_of(x * 256, 256), 256)]
 
-    pl.semaphore_wait(barrier, 31 + 31 + 32 - has_self.astype(jnp.int32))
+    pl.semaphore_wait(barrier, 31 + 16)
+    for step in (2, 6):
+        pl.semaphore_signal(
+            far_sem, inc=1, device_id=((z + step) % NZ * NX + x, t), device_id_type=MESH
+        )
 
     def send_tokens(i, c):
         px, pt = in_plane(i)
@@ -220,6 +231,9 @@
     lax.fori_loop(0, 3, send_first, 0)
     lax.fori_loop(0, 31, send_tokens, 0)
 
+    leaving.append((tok_all.at[pl.ds(0, 31)], 0))
+    leaving.append((gains.at[pl.ds(0, 3)], 1))
+    leaving.append((w_first.at[pl.ds(0, 3)], 2))
     wait_for(gains.at[pl.ds(0, 3)], recv_sems.at[1])
     wait_for(tok_all.at[pl.ds(0, 31)], recv_sems.at[0])
 
@@ -230,6 +244,7 @@
         return c
 
     lax.fori_loop(0, 7, send_wout, 0)
+    leaving.append((w_out.at[pl.ds(0, 7)], 3))
 
     raw = [
         tok_all[pl.ds(NT * q, NT)].astype(F32).reshape(192, 128) for q in range(NX)
@@ -251,6 +266,8 @@
                 [left[12:24], right[12:24]], axis=0
             ).astype(BF16)
 
+    pl.semaphore_wait(far_sem, 2)
+
     def send_sq1(i, c):
         pz = (z + far_first(i, 8)) % 8
         copy_to(sq1.at[z], sq1.at[z], 4, pz * NX + x, t).start()
@@ -264,6 +281,8 @@
     lax.fori_loop(0, 7, send_sq1, 0)
     lax.fori_loop(0, 31, send_proj, 0)
     proj_in[kv] = proj_out[kv]
+    leaving.append((sq1.at[pl.ds(0, 7)], 4))
+    leaving.append((proj_in.at[pl.ds(0, 31)], 5))
 
     def send_ffn(i, c):
         px = (x + far_first(i, 4)) % 4
@@ -273,6 +292,8 @@
         return c
 
     lax.fori_loop(0, 3, send_ffn, 0)
+    leaving.append((w_up.at[pl.ds(0, 3)], 6))
+    leaving.append((w_down.at[pl.ds(0, 3)], 7))
 
     for k in range(9, 12):
         loads[k].wait()
@@ -306,8 +327,6 @@
         nxt = f * state_v[s, h] + (1.0 - f) * values_in[j : j + 1, :]
         next_v[s, h] = nxt
         read_v[j : j + 1, :] = jnp.sum(queries_t[:, j : j + 1] * nxt, axis=0, keepdims=True)
-    store = pltpu.make_async_copy(next_v, next_hbm, in_sems.at[12])
-    store.start()
     read = read_v[...]
     read = read * lax.rsqrt(jnp.mean(read * read, axis=1, keepdims=True) + NORM_EPS) * head_gain
     mix_own[...] = (read * jax.nn.silu(gate_raw)).astype(BF16)
@@ -329,6 +348,7 @@
     def _():
         mix_all[t * NX + x] = mix_own[...]
 
+    mix_sent.append(1)
     wait_for(w_out.at[pl.ds(0, 7)], recv_sems.at[3])
 
     @pl.when(has_self)
@@ -361,6 +381,7 @@
         return c
 
     lax.fori_loop(0, 31, send_mixed, 0)
+    leaving.append((mixed_all.at[pl.ds(0, 31)], 9))
     wait_for(w_up.at[pl.ds(0, 3)], recv_sems.at[6])
     wait_for(mixed_all.at[pl.ds(0, 31)], recv_sems.at[9])
 
@@ -383,6 +404,8 @@
 
     lax.fori_loop(0, 7, send_up, 0)
     up_in[z] = up_out[z]
+    leaving.append((sq2.at[pl.ds(0, 7)], 10))
+    leaving.append((up_in.at[pl.ds(0, 7)], 11))
     wait_for(sq2.at[pl.ds(0, 7)], recv_sems.at[10])
     squares2 = sq2[0]
     for q in range(1, NZ):
@@ -406,6 +429,7 @@
         return c
 
     lax.fori_loop(0, 7, send_hidden, 0)
+    leaving.append((hidden_all.at[pl.ds(0, 7)], 12))
     wait_for(w_down.at[pl.ds(0, 3)], recv_sems.at[7])
     wait_for(hidden_all.at[pl.ds(0, 7)], recv_sems.at[12])
 
@@ -428,6 +452,7 @@
 
     lax.fori_loop(0, 31, send_down, 0)
     down_in[t * NX + x] = down_out[t * NX + x]
+    leaving.append((down_in.at[pl.ds(0, 31)], 13))
     wait_for(down_in.at[pl.ds(0, 31)], recv_sems.at[13])
     total = down_in[0].astype(F32)
     for q in range(1, 32):
@@ -435,29 +460,7 @@
     total = mixed_all[x * NT + t].astype(F32) + total
     out_ref[...] = jnp.concatenate([total[:, 0:64], total[:, 64:128]], axis=0).astype(BF16)
 
-    store.wait()
-    wait_for(tok_all.at[pl.ds(0, 31)], send_sems.at[0])
-    wait_for(gains.at[pl.ds(0, 3)], send_sems.at[1])
-    wait_for(w_first.at[pl.ds(0, 3)], send_sems.at[2])
-    wait_for(w_out.at[pl.ds(0, 7)], send_sems.at[3])
-    wait_for(sq1.at[pl.ds(0, 7)], send_sems.at[4])
-    wait_for(proj_in.at[pl.ds(0, 31)], send_sems.at[5])
-    wait_for(w_up.at[pl.ds(0, 3)], send_sems.at[6])
-    wait_for(w_down.at[pl.ds(0, 3)], send_sems.at[7])
-
-    @pl.when(has_self)
-    def _():
-        wait_for(mix_all.at[pl.ds(0, 31)], send_sems.at[8])
-
-    @pl.when(jnp.logical_not(has_self))
-    def _():
-        wait_for(mix_all, send_sems.at[8])
-
-    wait_for(mixed_all.at[pl.ds(0, 31)], send_sems.at[9])
-    wait_for(sq2.at[pl.ds(0, 7)], send_sems.at[10])
-    wait_for(up_in.at[pl.ds(0, 7)], send_sems.at[11])
-    wait_for(hidden_all.at[pl.ds(0, 7)], send_sems.at[12])
-    wait_for(down_in.at[pl.ds(0, 31)], send_sems.at[13])
+    finish()
 
 
 def body(
@@ -475,24 +478,23 @@
     w_up,
     w_down,
 ):
-    gains = jnp.stack([norm_gain, mixer_gain])
     bound = lower_bound.reshape(2, 128)
-    any_spec = pl.BlockSpec(memory_space=pl.ANY)
+    any_spec = pl.BlockSpec(memory_space=pltpu.HBM)
+    vmem_spec = pl.BlockSpec(memory_space=pltpu.VMEM)
     return pl.pallas_call(
         kernel,
         out_shape=(
             jax.ShapeDtypeStruct(tokens.shape, tokens.dtype),
             jax.ShapeDtypeStruct(recur_state.shape, recur_state.dtype),
         ),
-        in_specs=[any_spec] * 12,
-        out_specs=(pl.BlockSpec(memory_space=pltpu.VMEM), any_spec),
+        in_specs=[any_spec] * 13,
+        out_specs=(vmem_spec, vmem_spec),
         scratch_shapes=[
             pltpu.VMEM((48, 64), BF16),
-            pltpu.VMEM((2, 64), F32),
+            pltpu.VMEM((2, 1, 64), F32),
             pltpu.VMEM((4, 64, 256), BF16),
             pltpu.VMEM((2, 128), F32),
             pltpu.VMEM((2, 128), F32),
-            pltpu.VMEM((12, 2, 128, 128), F32),
             pltpu.VMEM((12, 2, 128, 128), F32),
             pltpu.VMEM((64, 256), BF16),
             pltpu.VMEM((64, 1024), BF16),
@@ -519,12 +521,14 @@
             pltpu.SemaphoreType.DMA((13,)),
             pltpu.SemaphoreType.DMA((14,)),
             pltpu.SemaphoreType.DMA((14,)),
+            pltpu.SemaphoreType.REGULAR,
         ],
-        compiler_params=pltpu.CompilerParams(collective_id=0, has_side_effects=True),
+        compiler_params=pltpu.CompilerParams(collective_id=0, has_side_effects=True, vmem_limit_bytes=16 * 1024 * 1024),
         name="decode_layer",
-    )(
+    )(*(pltpu.with_memory_space_constraint(a, pltpu.HBM) for a in (
         tokens,
-        gains,
+        norm_gain.reshape(1, 64),
+        mixer_gain.reshape(1, 64),
         w_query,
         w_forget,
         w_input,
@@ -535,7 +539,7 @@
         w_out.T,
         w_up,
         w_down.T,
-    )
+    )))
 
 
 def solution(mesh):

time: 71.4 us -> 66.2 us (0.927)
  local copies, waits for them, and re-layouts: 4.01 us -> 1.74 us
  Pallas kernels: 65.2 us -> 63.6 us
  other arithmetic: 1.24 us -> 0 us
    unnamed x2, local copies, waits for them, and re-layouts: 4.01 us -> 1.74 us
    pallas_call x1, Pallas kernels: 65.2 us -> 63.6 us  [body(): pl.pallas_call(kernel, out_shape=(jax.ShapeDtypeStruct(tokens.shape, toke...]
    another operation x1 -> x0, other arithmetic: 1.24 us -> none  [body(): gains = jnp.stack([norm_gain, mixer_gain])]
where the time goes in v2:
time: 66.2 us; the launch traced here: 66 us
  Pallas kernels  63.6 us (96%)
  local copies, waits for them, and re-layouts  1.74 us (3%)
    pallas_call x1, Pallas kernels, body(): pl.pallas_call(kernel, out_shape=(jax.ShapeDtypeStruct(tokens.shape, toke...  63.6 us
    unnamed x2, local copies, waits for them, and re-layouts  1.74 us

profile of v2, /device:TPU:1, one launch (start us, length us, event | category | flops | bytes accessed | tf_op | source)
XLA Modules:
  0.0 66.0 jit_solution(8056279449507553168)
XLA Ops:
  0.6 63.6 %decode_layer.1 = (bf16[48,64]{1,0:T(8,128)(2,1)S(1)}, f32[12,2,128,128]{3,2,1,0:T(8,128)S(1)}) custom-call(bf16[48,64]{1,0:T(8,128)(2,1)} %tokens_hbm.1, f32[1,64]{1,0:T(1,128)} %bitcast.8, f32[1,64]{1,0:T(1,128)} %bitcast.9, bf16[64,256]{1,0:T(8,128)(2,1)} %wq_hbm.1, bf16[64,256]{1,0:T(8,128)(2,1)} %wf_hbm.1, bf16[64,256]{1,0:T(8,128)(2,1)} %wi_hbm.1, ...), custom_call_target="tpu_custom_call" | custom-call | tf_op jit(solution)/shard_map/decode_layer/pallas_call | solution.py:484
  64.3 0.6 copy.17
  64.9 1.1 %copy.18 = f32[12,2,128,128]{3,2,1,0:T(8,128)} copy(f32[12,2,128,128]{3,2,1,0:T(8,128)S(1)} %get-tuple-element.5) | data formatting | bytes 3145728

commit v3 on v2

--- a/solution.py
+++ b/solution.py
@@ -1,4 +1,4 @@
-import functools
+import itertools
 
 import jax
 import jax.numpy as jnp
@@ -16,8 +16,20 @@
 WIDTH = 2048.0
 
 
-def far_first(step, size):
-    return ((step + 1) // 2) * (1 - 2 * (step % 2)) + size // 2
+def hops(step, size):
+    return min(step, size - step)
+
+
+def by_distance(sizes):
+    steps = list(itertools.product(*(range(n) for n in sizes)))[1:]
+    return sorted(steps, key=lambda d: (-sum(hops(s, n) for s, n in zip(d, sizes)), d))
+
+
+PLANE = by_distance((4, 4, 2))
+COLUMN = by_distance((8, 4))
+ALONG_X = by_distance((4,))
+ALONG_Y = by_distance((4, 2))
+ALONG_Z = by_distance((8,))
 
 
 def wait_for(ref, sem):
@@ -125,16 +137,12 @@
     rows_at = (t + NZ - z) % NZ
     has_self = t == (2 * z) % NZ
 
-    def in_plane(i):
-        px = (x + far_first(i // 8, 4)) % 4
-        py = (y + far_first((i % 8) // 2, 4)) % 4
-        pc = (core + 1 - i % 2) % 2
-        return px, 2 * py + pc
-
-    def in_column(i):
-        pz = (z + far_first(i // 4, 8)) % 8
-        px = (x + far_first(i % 4, 4)) % 4
-        return pz, px
+    xs = [(x + d) % 4 for d in range(4)]
+    ys = [(y + d) % 4 for d in range(4)]
+    zs = [(z + d) % 8 for d in range(8)]
+    cores = [core, 1 - core]
+    kvs = [[pz * NX + px for px in xs] for pz in zs]
+    ts = [[2 * py + pc for pc in cores] for py in ys]
 
     def copy_to(src, dst, k, pkv, pt):
         return pltpu.make_async_remote_copy(
@@ -165,18 +173,11 @@
     def tell(pkv, pt):
         pl.semaphore_signal(barrier, inc=1, device_id=(pkv, pt), device_id_type=MESH)
 
-    def greet_plane(i, c):
-        px, pt = in_plane(i)
-        tell(z * NX + px, pt)
-        return c
-
-    def greet_near(i, c):
-        pz = (z + (i // 8 + 1) * (1 - 2 * ((i // 4) % 2)) + NZ) % NZ
-        tell(pz * NX + (x + i) % NX, t)
-        return c
-
-    lax.fori_loop(0, 31, greet_plane, 0)
-    lax.fori_loop(0, 16, greet_near, 0)
+    for dx, dy, dc in PLANE:
+        tell(kvs[0][dx], ts[dy][dc])
+    for dz in (2, 6, 1, 7):
+        for dx in (2, 1, 3, 0):
+            tell(kvs[dz][dx], t)
 
     loads = [
         pltpu.make_async_copy(tokens_hbm, tok_v, in_sems.at[0]),
@@ -214,36 +215,23 @@
     pl.semaphore_wait(barrier, 31 + 16)
     for step in (2, 6):
         pl.semaphore_signal(
-            far_sem, inc=1, device_id=((z + step) % NZ * NX + x, t), device_id_type=MESH
+            far_sem, inc=1, device_id=(kvs[step][0], t), device_id_type=MESH
         )
 
-    def send_tokens(i, c):
-        px, pt = in_plane(i)
-        copy_to(tok_all.at[x * NT + t], tok_all.at[x * NT + t], 0, z * NX + px, pt).start()
-        return c
-
-    def send_first(i, c):
-        px = (x + far_first(i, 4)) % 4
-        copy_to(gains.at[x], gains.at[x], 1, z * NX + px, t).start()
-        copy_to(w4_v.at[px], w_first.at[x], 2, z * NX + px, t).start()
-        return c
-
-    lax.fori_loop(0, 3, send_first, 0)
-    lax.fori_loop(0, 31, send_tokens, 0)
-
+    for (dx,) in ALONG_X:
+        copy_to(gains.at[x], gains.at[x], 1, kvs[0][dx], t).start()
+        copy_to(w4_v.at[xs[dx]], w_first.at[x], 2, kvs[0][dx], t).start()
+    own_tok = tok_all.at[x * NT + t]
+    for dx, dy, dc in PLANE:
+        copy_to(own_tok, own_tok, 0, kvs[0][dx], ts[dy][dc]).start()
     leaving.append((tok_all.at[pl.ds(0, 31)], 0))
     leaving.append((gains.at[pl.ds(0, 3)], 1))
     leaving.append((w_first.at[pl.ds(0, 3)], 2))
     wait_for(gains.at[pl.ds(0, 3)], recv_sems.at[1])
     wait_for(tok_all.at[pl.ds(0, 31)], recv_sems.at[0])
 
-    def send_wout(i, c):
-        py = (y + far_first(i // 2, 4)) % 4
-        pt = 2 * py + (core + 1 - i % 2) % 2
-        copy_to(w_out.at[t], w_out.at[t], 3, kv, pt).start()
-        return c
-
-    lax.fori_loop(0, 7, send_wout, 0)
+    for dy, dc in ALONG_Y:
+        copy_to(w_out.at[t], w_out.at[t], 3, kv, ts[dy][dc]).start()
     leaving.append((w_out.at[pl.ds(0, 7)], 3))
 
     raw = [
@@ -268,30 +256,18 @@
 
     pl.semaphore_wait(far_sem, 2)
 
-    def send_sq1(i, c):
-        pz = (z + far_first(i, 8)) % 8
-        copy_to(sq1.at[z], sq1.at[z], 4, pz * NX + x, t).start()
-        return c
-
-    def send_proj(i, c):
-        pz, px = in_column(i)
-        copy_to(proj_out.at[pz * NX + px], proj_in.at[kv], 5, pz * NX + px, t).start()
-        return c
-
-    lax.fori_loop(0, 7, send_sq1, 0)
-    lax.fori_loop(0, 31, send_proj, 0)
+    for (dz,) in ALONG_Z:
+        copy_to(sq1.at[z], sq1.at[z], 4, kvs[dz][0], t).start()
+    for dz, dx in COLUMN:
+        copy_to(proj_out.at[kvs[dz][dx]], proj_in.at[kv], 5, kvs[dz][dx], t).start()
     proj_in[kv] = proj_out[kv]
     leaving.append((sq1.at[pl.ds(0, 7)], 4))
     leaving.append((proj_in.at[pl.ds(0, 31)], 5))
 
-    def send_ffn(i, c):
-        px = (x + far_first(i, 4)) % 4
-        cols = pl.ds(pl.multiple_of(px * 256, 256), 256)
-        copy_to(wup_v.at[:, cols], w_up.at[x], 6, z * NX + px, t).start()
-        copy_to(wdown_v.at[:, cols], w_down.at[x], 7, z * NX + px, t).start()
-        return c
-
-    lax.fori_loop(0, 3, send_ffn, 0)
+    for (dx,) in ALONG_X:
+        cols = pl.ds(pl.multiple_of(xs[dx] * 256, 256), 256)
+        copy_to(wup_v.at[:, cols], w_up.at[x], 6, kvs[0][dx], t).start()
+        copy_to(wdown_v.at[:, cols], w_down.at[x], 7, kvs[0][dx], t).start()
     leaving.append((w_up.at[pl.ds(0, 3)], 6))
     leaving.append((w_down.at[pl.ds(0, 3)], 7))
 
@@ -319,36 +295,34 @@
     head_gain = jnp.where(head0, head_gain_v[0:1, :], head_gain_v[1:2, :])
     forget = bound + (1.0 - bound) * jax.nn.sigmoid(forget_raw)
     pad = jnp.zeros((104, 128), F32)
-    forget_t = jnp.concatenate([forget, pad], axis=0).T
-    queries_t = jnp.concatenate([queries, pad], axis=0).T
+    kept = queries * forget
+    kept_t = jnp.concatenate([kept, pad], axis=0).T
+    fresh = jnp.sum(queries * (1.0 - forget), axis=1, keepdims=True) * values_in
     for j in range(24):
-        h, s = j // 12, j % 12
-        f = forget_t[:, j : j + 1]
-        nxt = f * state_v[s, h] + (1.0 - f) * values_in[j : j + 1, :]
-        next_v[s, h] = nxt
-        read_v[j : j + 1, :] = jnp.sum(queries_t[:, j : j + 1] * nxt, axis=0, keepdims=True)
-    read = read_v[...]
+        read_v[j : j + 1, :] = jnp.sum(
+            kept_t[:, j : j + 1] * state_v[j % 12, j // 12], axis=0, keepdims=True
+        )
+    read = read_v[...] + fresh
     read = read * lax.rsqrt(jnp.mean(read * read, axis=1, keepdims=True) + NORM_EPS) * head_gain
     mix_own[...] = (read * jax.nn.silu(gate_raw)).astype(BF16)
 
-    def send_mix(i, c):
-        pz, px = (z + far_first(i // 4, 8)) % 8, (x + far_first(i % 4, 4)) % 4
-        pt = (z + pz) % NZ
-        away = jnp.logical_or(pz * NX + px != kv, pt != t)
-
-        @pl.when(away)
-        def _():
-            copy_to(mix_own, mix_all.at[t * NX + x], 8, pz * NX + px, pt).start()
-
-        return c
-
-    lax.fori_loop(0, 32, send_mix, 0)
+    mix_at = t * NX + x
+    for dz, dx in COLUMN:
+        copy_to(mix_own, mix_all.at[mix_at], 8, kvs[dz][dx], (z + zs[dz]) % NZ).start()
+
+    @pl.when(jnp.logical_not(has_self))
+    def _():
+        copy_to(mix_own, mix_all.at[mix_at], 8, kv, (2 * z) % NZ).start()
 
     @pl.when(has_self)
     def _():
-        mix_all[t * NX + x] = mix_own[...]
+        mix_all[mix_at] = mix_own[...]
 
     mix_sent.append(1)
+    forget_t = jnp.concatenate([forget, pad], axis=0).T
+    for j in range(24):
+        f = forget_t[:, j : j + 1]
+        next_v[j % 12, j // 12] = f * state_v[j % 12, j // 12] + (1.0 - f) * values_in[j : j + 1, :]
     wait_for(w_out.at[pl.ds(0, 7)], recv_sems.at[3])
 
     @pl.when(has_self)
@@ -375,12 +349,8 @@
     own_at = x * NT + rows_at
     mixed_all[own_at] = (tok_all[own_at].astype(F32) + attn).astype(BF16)
 
-    def send_mixed(i, c):
-        px, pt = in_plane(i)
-        copy_to(mixed_all.at[own_at], mixed_all.at[own_at], 9, z * NX + px, pt).start()
-        return c
-
-    lax.fori_loop(0, 31, send_mixed, 0)
+    for dx, dy, dc in PLANE:
+        copy_to(mixed_all.at[own_at], mixed_all.at[own_at], 9, kvs[0][dx], ts[dy][dc]).start()
     leaving.append((mixed_all.at[pl.ds(0, 31)], 9))
     wait_for(w_up.at[pl.ds(0, 3)], recv_sems.at[6])
     wait_for(mixed_all.at[pl.ds(0, 31)], recv_sems.at[9])
@@ -396,13 +366,9 @@
             at = half * 192 + pz * 24
             up_out[pz, half] = partial2[at : at + 24].astype(BF16)
 
-    def send_up(i, c):
-        pz = (z + far_first(i, 8)) % 8
-        copy_to(sq2.at[z], sq2.at[z], 10, pz * NX + x, t).start()
-        copy_to(up_out.at[pz], up_in.at[z], 11, pz * NX + x, t).start()
-        return c
-
-    lax.fori_loop(0, 7, send_up, 0)
+    for (dz,) in ALONG_Z:
+        copy_to(sq2.at[z], sq2.at[z], 10, kvs[dz][0], t).start()
+        copy_to(up_out.at[zs[dz]], up_in.at[z], 11, kvs[dz][0], t).start()
     up_in[z] = up_out[z]
     leaving.append((sq2.at[pl.ds(0, 7)], 10))
     leaving.append((up_in.at[pl.ds(0, 7)], 11))
@@ -423,12 +389,8 @@
         total = jnp.maximum(total * scales[half], 0.0)
         hidden_all[z, half] = (total * total).astype(BF16)
 
-    def send_hidden(i, c):
-        pz = (z + far_first(i, 8)) % 8
-        copy_to(hidden_all.at[z], hidden_all.at[z], 12, pz * NX + x, t).start()
-        return c
-
-    lax.fori_loop(0, 7, send_hidden, 0)
+    for (dz,) in ALONG_Z:
+        copy_to(hidden_all.at[z], hidden_all.at[z], 12, kvs[dz][0], t).start()
     leaving.append((hidden_all.at[pl.ds(0, 7)], 12))
     wait_for(w_down.at[pl.ds(0, 3)], recv_sems.at[7])
     wait_for(hidden_all.at[pl.ds(0, 7)], recv_sems.at[12])
@@ -443,14 +405,14 @@
                 BF16
             )
 
-    def send_down(i, c):
-        px, pt = in_plane(i)
+    for dx, dy, dc in PLANE:
         copy_to(
-            down_out.at[pt * NX + px], down_in.at[t * NX + x], 13, z * NX + px, pt
+            down_out.at[ts[dy][dc] * NX + xs[dx]],
+            down_in.at[t * NX + x],
+            13,
+            kvs[0][dx],
+            ts[dy][dc],
         ).start()
-        return c
-
-    lax.fori_loop(0, 31, send_down, 0)
     down_in[t * NX + x] = down_out[t * NX + x]
     leaving.append((down_in.at[pl.ds(0, 31)], 13))
     wait_for(down_in.at[pl.ds(0, 31)], recv_sems.at[13])

time: 66.2 us -> 61.1 us (0.923)
  Pallas kernels: 63.6 us -> 58.6 us
    pallas_call x1, Pallas kernels: 63.6 us -> 58.6 us  [body(): pl.pallas_call(kernel, out_shape=(jax.ShapeDtypeStruct(tokens.shape, toke...]
where the time goes in v3:
time: 61.1 us; the launch traced here: 61 us
  Pallas kernels  58.6 us (96%)
  local copies, waits for them, and re-layouts  1.74 us (3%)
  between operations  0.64 us (1%)
    pallas_call x1, Pallas kernels, body(): pl.pallas_call(kernel, out_shape=(jax.ShapeDtypeStruct(tokens.shape, toke...  58.6 us
    unnamed x2, local copies, waits for them, and re-layouts  1.74 us

profile of v3, /device:TPU:1, one launch (start us, length us, event | category | flops | bytes accessed | tf_op | source)
XLA Modules:
  0.0 61.0 jit_solution(10329942393168879942)
XLA Ops:
  0.6 58.6 %decode_layer.1 = (bf16[48,64]{1,0:T(8,128)(2,1)S(1)}, f32[12,2,128,128]{3,2,1,0:T(8,128)S(1)}) custom-call(bf16[48,64]{1,0:T(8,128)(2,1)} %tokens_hbm.1, f32[1,64]{1,0:T(1,128)} %bitcast.8, f32[1,64]{1,0:T(1,128)} %bitcast.9, bf16[64,256]{1,0:T(8,128)(2,1)} %wq_hbm.1, bf16[64,256]{1,0:T(8,128)(2,1)} %wf_hbm.1, bf16[64,256]{1,0:T(8,128)(2,1)} %wi_hbm.1, ...), custom_call_target="tpu_custom_call" | custom-call | tf_op jit(solution)/shard_map/decode_layer/pallas_call | solution.py:446
  59.3 0.6 copy.17
  59.9 1.1 %copy.18 = f32[12,2,128,128]{3,2,1,0:T(8,128)} copy(f32[12,2,128,128]{3,2,1,0:T(8,128)S(1)} %get-tuple-element.5) | data formatting | bytes 3145728

commit v4 on v3

--- a/solution.py
+++ b/solution.py
@@ -14,6 +14,7 @@
 
 NZ, NX, NT = 8, 4, 8
 WIDTH = 2048.0
+FIRST_TOKENS = 16
 
 
 def hops(step, size):
@@ -30,6 +31,8 @@
 ALONG_X = by_distance((4,))
 ALONG_Y = by_distance((4, 2))
 ALONG_Z = by_distance((8,))
+NEAR_Y = [(0, 0)] + ALONG_Y[::-1]
+NEAR_Z = [0, 1, 7, 2, 6, 3, 5, 4]
 
 
 def wait_for(ref, sem):
@@ -51,32 +54,30 @@
 def unpacked(pieces):
     low = low_lanes(pieces[0].shape)
     swapped = [swap_lanes(p) for p in pieces]
-    first = [jnp.where(low, pieces[i], swapped[i + 1]).astype(BF16) for i in (0, 2)]
-    second = [jnp.where(low, swapped[i], pieces[i + 1]).astype(BF16) for i in (0, 2)]
+    first = [jnp.where(low, pieces[i], swapped[i + 1]) for i in (0, 2)]
+    second = [jnp.where(low, swapped[i], pieces[i + 1]) for i in (0, 2)]
     return jnp.concatenate(
         [jnp.concatenate(first, axis=1), jnp.concatenate(second, axis=1)], axis=0
-    )
+    ).astype(BF16)
 
 
 def row_squares(pieces):
     total = pieces[0] * pieces[0]
     for p in pieces[1:]:
         total = total + p * p
-    total = jnp.concatenate([total, jnp.zeros((64, 128), F32)], axis=0)
+    total = jnp.concatenate([total, jnp.zeros((104, 128), F32)], axis=0)
     high = total.astype(BF16)
     rest = (total - high.astype(F32)).astype(BF16)
     lane = lax.broadcasted_iota(jnp.int32, (8, 128), 1)
     row = lax.broadcasted_iota(jnp.int32, (8, 128), 0)
     pick = jnp.where((lane // 64) == row, 1.0, 0.0).astype(BF16)
-    dims = (((1,), (1,)), ((), ()))
-    sums = lax.dot_general(pick, high, dims, preferred_element_type=F32)
-    sums = sums + lax.dot_general(pick, rest, dims, preferred_element_type=F32)
+    sums = dot_t(pick, high) + dot_t(pick, rest)
     return sums[0:2, :]
 
 
 def column_of(values, base, period):
-    lane = lax.broadcasted_iota(jnp.int32, (24, 256), 1)
-    row = lax.broadcasted_iota(jnp.int32, (24, 256), 0)
+    lane = lax.broadcasted_iota(jnp.int32, (24, 128), 1)
+    row = lax.broadcasted_iota(jnp.int32, (24, 128), 0)
     return jnp.sum(
         jnp.where(lane == base + row % period, values, 0.0), axis=1, keepdims=True
     )
@@ -113,15 +114,18 @@
     w_down,
     w_out,
     tok_all,
+    sq_out,
     sq1,
     proj_out,
     proj_in,
     mix_own,
     mix_all,
     mixed_all,
+    sq_out2,
     sq2,
     up_out,
     up_in,
+    hidden_own,
     hidden_all,
     down_out,
     down_in,
@@ -129,6 +133,9 @@
     in_sems,
     send_sems,
     recv_sems,
+    tok_sems,
+    mixed_sems,
+    hidden_sems,
     far_sem,
 ):
     kv, t = lax.axis_index("kv"), lax.axis_index("tp")
@@ -143,13 +150,14 @@
     cores = [core, 1 - core]
     kvs = [[pz * NX + px for px in xs] for pz in zs]
     ts = [[2 * py + pc for pc in cores] for py in ys]
-
-    def copy_to(src, dst, k, pkv, pt):
+    sibling = ts[0][1]
+
+    def copy_to(src, dst, k, pkv, pt, arrived=None):
         return pltpu.make_async_remote_copy(
             src_ref=src,
             dst_ref=dst,
             send_sem=send_sems.at[k],
-            recv_sem=recv_sems.at[k],
+            recv_sem=recv_sems.at[k] if arrived is None else arrived,
             device_id=(pkv, pt),
             device_id_type=MESH,
         )
@@ -177,7 +185,9 @@
         tell(kvs[0][dx], ts[dy][dc])
     for dz in (2, 6, 1, 7):
         for dx in (2, 1, 3, 0):
-            tell(kvs[dz][dx], t)
+            tell(kvs[dz][dx], sibling)
+    for dz in (2, 6):
+        tell(kvs[dz][0], t)
 
     loads = [
         pltpu.make_async_copy(tokens_hbm, tok_v, in_sems.at[0]),
@@ -207,62 +217,62 @@
         gains[x, q : q + 1, :] = jnp.concatenate([g, g], axis=1)
     for k in range(2, 9):
         loads[k].wait()
-    w_first[x] = w4_v[x]
     w_up[x] = wup_v[:, pl.ds(pl.multiple_of(x * 256, 256), 256)]
     w_out[t] = wout_v[...]
     w_down[x] = wdown_v[:, pl.ds(pl.multiple_of(x * 256, 256), 256)]
 
-    pl.semaphore_wait(barrier, 31 + 16)
+    pl.semaphore_wait(barrier, 31 + 16 + 2)
     for step in (2, 6):
         pl.semaphore_signal(
             far_sem, inc=1, device_id=(kvs[step][0], t), device_id_type=MESH
         )
 
+    own_tok = tok_all.at[x * NT + t]
+
+    def send_tokens(steps):
+        for dx, dy, dc in steps:
+            copy_to(own_tok, own_tok, 0, kvs[0][dx], ts[dy][dc], tok_sems.at[t]).start()
+
+    send_tokens(PLANE[:FIRST_TOKENS])
     for (dx,) in ALONG_X:
         copy_to(gains.at[x], gains.at[x], 1, kvs[0][dx], t).start()
-        copy_to(w4_v.at[xs[dx]], w_first.at[x], 2, kvs[0][dx], t).start()
-    own_tok = tok_all.at[x * NT + t]
-    for dx, dy, dc in PLANE:
-        copy_to(own_tok, own_tok, 0, kvs[0][dx], ts[dy][dc]).start()
+    for dx in (2, 1, 3, 0):
+        copy_to(w4_v.at[xs[dx]], w_first.at[x], 2, kvs[0][dx], sibling).start()
+    send_tokens(PLANE[FIRST_TOKENS:])
     leaving.append((tok_all.at[pl.ds(0, 31)], 0))
     leaving.append((gains.at[pl.ds(0, 3)], 1))
-    leaving.append((w_first.at[pl.ds(0, 3)], 2))
-    wait_for(gains.at[pl.ds(0, 3)], recv_sems.at[1])
-    wait_for(tok_all.at[pl.ds(0, 31)], recv_sems.at[0])
+    leaving.append((w_first, 2))
 
     for dy, dc in ALONG_Y:
         copy_to(w_out.at[t], w_out.at[t], 3, kv, ts[dy][dc]).start()
     leaving.append((w_out.at[pl.ds(0, 7)], 3))
 
-    raw = [
-        tok_all[pl.ds(NT * q, NT)].astype(F32).reshape(192, 128) for q in range(NX)
-    ]
-    sq1[z] = row_squares(raw)
-    lhs = unpacked([raw[q] * gains[q, 0:1, :] for q in range(NX)])
-    wait_for(w_first.at[pl.ds(0, 3)], recv_sems.at[2])
-    partial = jnp.dot(lhs, w_first[...].reshape(256, 256), preferred_element_type=F32)
-
-    for half in range(2):
-        for pz in range(NZ):
-            at = half * 192 + pz * 24
-            left = partial[at : at + 24, 0:128]
-            right = partial[at : at + 24, 128:256]
+    wait_for(gains.at[pl.ds(0, 3)], recv_sems.at[1])
+    wait_for(w_first, recv_sems.at[2])
+
+    pl.semaphore_wait(far_sem, 2)
+    for dy, dc in NEAR_Y:
+        pz = ts[dy][dc]
+        wait_for(tok_all.at[pl.ds(0, 3 if dy == dc == 0 else 4)], tok_sems.at[pz])
+        raw = [tok_all[q * NT + pz].astype(F32) for q in range(NX)]
+        lhs = unpacked([raw[q] * gains[q, 0:1, :] for q in range(NX)])
+        partial = jnp.dot(lhs, w_first[...].reshape(256, 256), preferred_element_type=F32)
+        for half in range(2):
+            left = partial[24 * half : 24 * half + 24, 0:128]
+            right = partial[24 * half : 24 * half + 24, 128:256]
             proj_out[pz * NX + 2 * half] = jnp.concatenate(
                 [left[0:12], right[0:12]], axis=0
             ).astype(BF16)
             proj_out[pz * NX + 2 * half + 1] = jnp.concatenate(
                 [left[12:24], right[12:24]], axis=0
             ).astype(BF16)
-
-    pl.semaphore_wait(far_sem, 2)
-
-    for (dz,) in ALONG_Z:
-        copy_to(sq1.at[z], sq1.at[z], 4, kvs[dz][0], t).start()
-    for dz, dx in COLUMN:
-        copy_to(proj_out.at[kvs[dz][dx]], proj_in.at[kv], 5, kvs[dz][dx], t).start()
-    proj_in[kv] = proj_out[kv]
-    leaving.append((sq1.at[pl.ds(0, 7)], 4))
-    leaving.append((proj_in.at[pl.ds(0, 31)], 5))
+        sq_out[pz] = row_squares(raw)
+        for dx in (2, 1, 3, 0):
+            to = pz * NX + xs[dx]
+            copy_to(proj_out.at[to], proj_in.at[kv], 5, to, sibling).start()
+        copy_to(sq_out.at[pz], sq1.at[z], 4, pz * NX + x, sibling).start()
+    leaving.append((sq1, 4))
+    leaving.append((proj_in, 5))
 
     for (dx,) in ALONG_X:
         cols = pl.ds(pl.multiple_of(xs[dx] * 256, 256), 256)
@@ -273,15 +283,15 @@
 
     for k in range(9, 12):
         loads[k].wait()
-    wait_for(sq1.at[pl.ds(0, 7)], recv_sems.at[4])
-    wait_for(proj_in.at[pl.ds(0, 31)], recv_sems.at[5])
+    wait_for(sq1, recv_sems.at[4])
+    wait_for(proj_in, recv_sems.at[5])
 
     squares = sq1[0]
     for q in range(1, NZ):
         squares = squares + sq1[q]
     square_row = jnp.where(x // 2 == 0, squares[0:1, :], squares[1:2, :])
     row_scale = lax.rsqrt(
-        column_of(square_row, z * 24 + (x % 2) * 12, 12) / WIDTH + NORM_EPS
+        column_of(square_row, (x % 2) * 12, 12) / WIDTH + NORM_EPS
     )
     owned = []
     for q in range(NX):
@@ -349,71 +359,70 @@
     own_at = x * NT + rows_at
     mixed_all[own_at] = (tok_all[own_at].astype(F32) + attn).astype(BF16)
 
+    own_mixed = mixed_all.at[own_at]
     for dx, dy, dc in PLANE:
-        copy_to(mixed_all.at[own_at], mixed_all.at[own_at], 9, kvs[0][dx], ts[dy][dc]).start()
+        copy_to(own_mixed, own_mixed, 9, kvs[0][dx], ts[dy][dc], mixed_sems.at[rows_at]).start()
     leaving.append((mixed_all.at[pl.ds(0, 31)], 9))
     wait_for(w_up.at[pl.ds(0, 3)], recv_sems.at[6])
-    wait_for(mixed_all.at[pl.ds(0, 31)], recv_sems.at[9])
-
-    raw2 = [
-        mixed_all[pl.ds(NT * q, NT)].astype(F32).reshape(192, 128) for q in range(NX)
-    ]
-    sq2[z] = row_squares(raw2)
-    lhs2 = unpacked([raw2[q] * gains[q, 1:2, :] for q in range(NX)])
-    partial2 = jnp.dot(lhs2, w_up[...].reshape(256, 256), preferred_element_type=F32)
-    for half in range(2):
-        for pz in range(NZ):
-            at = half * 192 + pz * 24
-            up_out[pz, half] = partial2[at : at + 24].astype(BF16)
-
-    for (dz,) in ALONG_Z:
-        copy_to(sq2.at[z], sq2.at[z], 10, kvs[dz][0], t).start()
-        copy_to(up_out.at[zs[dz]], up_in.at[z], 11, kvs[dz][0], t).start()
-    up_in[z] = up_out[z]
-    leaving.append((sq2.at[pl.ds(0, 7)], 10))
-    leaving.append((up_in.at[pl.ds(0, 7)], 11))
-    wait_for(sq2.at[pl.ds(0, 7)], recv_sems.at[10])
+
+    for dy, dc in NEAR_Y:
+        pz = (ts[dy][dc] + NZ - z) % NZ
+        wait_for(mixed_all.at[pl.ds(0, 3 if dy == dc == 0 else 4)], mixed_sems.at[pz])
+        raw = [mixed_all[q * NT + pz].astype(F32) for q in range(NX)]
+        lhs = unpacked([raw[q] * gains[q, 1:2, :] for q in range(NX)])
+        partial = jnp.dot(lhs, w_up[...].reshape(256, 256), preferred_element_type=F32)
+        up_out[pz] = partial.reshape(2, 24, 256).astype(BF16)
+        sq_out2[pz] = row_squares(raw)
+        copy_to(up_out.at[pz], up_in.at[z], 11, pz * NX + x, sibling).start()
+        copy_to(sq_out2.at[pz], sq2.at[z], 10, pz * NX + x, sibling).start()
+    leaving.append((sq2, 10))
+    leaving.append((up_in, 11))
+    wait_for(sq2, recv_sems.at[10])
     squares2 = sq2[0]
     for q in range(1, NZ):
         squares2 = squares2 + sq2[q]
     scales = [
-        lax.rsqrt(column_of(squares2[q : q + 1, :], z * 24, 24) / WIDTH + NORM_EPS)
-        for q in range(2)
+        lax.rsqrt(column_of(squares2[q : q + 1, :], 0, 24) / WIDTH + NORM_EPS) for q in range(2)
     ]
-    wait_for(up_in.at[pl.ds(0, 7)], recv_sems.at[11])
+    wait_for(up_in, recv_sems.at[11])
 
     for half in range(2):
         total = up_in[0, half].astype(F32)
         for q in range(1, NZ):
             total = total + up_in[q, half].astype(F32)
         total = jnp.maximum(total * scales[half], 0.0)
-        hidden_all[z, half] = (total * total).astype(BF16)
-
-    for (dz,) in ALONG_Z:
-        copy_to(hidden_all.at[z], hidden_all.at[z], 12, kvs[dz][0], t).start()
-    leaving.append((hidden_all.at[pl.ds(0, 7)], 12))
+        hidden_own[half] = (total * total).astype(BF16)
+
+    for dz in NEAR_Z[::-1]:
+        copy_to(hidden_own, hidden_all.at[z], 12, kvs[dz][0], sibling, hidden_sems.at[z]).start()
+    leaving.append((hidden_all, 12))
     wait_for(w_down.at[pl.ds(0, 3)], recv_sems.at[7])
-    wait_for(hidden_all.at[pl.ds(0, 7)], recv_sems.at[12])
-
-    partial3 = dot_t(hidden_all[...].reshape(384, 256), w_down[...].reshape(256, 256))
-    for pt in range(NT):
+
+    down_at = t * NX + x
+    for dz in NEAR_Z:
+        pt = zs[dz]
+        wait_for(hidden_all.at[pt], hidden_sems.at[pt])
+        partial = dot_t(hidden_all[pt].reshape(48, 256), w_down[...].reshape(256, 256))
         for pair in range(2):
-            upper = partial3[48 * pt : 48 * pt + 24, 128 * pair : 128 * pair + 128]
-            lower = partial3[48 * pt + 24 : 48 * pt + 48, 128 * pair : 128 * pair + 128]
+            upper = partial[0:24, 128 * pair : 128 * pair + 128]
+            lower = partial[24:48, 128 * pair : 128 * pair + 128]
             down_out[pt * NX + 2 * pair] = jnp.where(low, upper, swap_lanes(lower)).astype(BF16)
             down_out[pt * NX + 2 * pair + 1] = jnp.where(low, swap_lanes(upper), lower).astype(
                 BF16
             )
-
-    for dx, dy, dc in PLANE:
-        copy_to(
-            down_out.at[ts[dy][dc] * NX + xs[dx]],
-            down_in.at[t * NX + x],
-            13,
-            kvs[0][dx],
-            ts[dy][dc],
-        ).start()
-    down_in[t * NX + x] = down_out[t * NX + x]
+        for dx in (2, 1, 3):
+            copy_to(
+                down_out.at[pt * NX + xs[dx]], down_in.at[down_at], 13, kvs[0][dx], pt
+            ).start()
+
+        @pl.when(pt != t)
+        def _():
+            copy_to(down_out.at[pt * NX + x], down_in.at[down_at], 13, kv, pt).start()
+
+        @pl.when(pt == t)
+        def _():
+            down_in[down_at] = down_out[down_at]
+
     leaving.append((down_in.at[pl.ds(0, 31)], 13))
     wait_for(down_in.at[pl.ds(0, 31)], recv_sems.at[13])
     total = down_in[0].astype(F32)
@@ -423,6 +432,20 @@
     out_ref[...] = jnp.concatenate([total[:, 0:64], total[:, 64:128]], axis=0).astype(BF16)
 
     finish()
+
+
+def place(out_v, next_v, out_hbm, next_hbm, sems):
+    copies = [
+        pltpu.make_async_copy(
+            next_v.at[pl.ds(2 * q, 2)], next_hbm.at[pl.ds(2 * q, 2)], sems.at[q]
+        )
+        for q in range(6)
+    ]
+    copies.append(pltpu.make_async_copy(out_v, out_hbm, sems.at[6]))
+    for copy in copies:
+        copy.start()
+    for copy in copies:
+        copy.wait()
 
 
 def body(
@@ -443,7 +466,7 @@
     bound = lower_bound.reshape(2, 128)
     any_spec = pl.BlockSpec(memory_space=pltpu.HBM)
     vmem_spec = pl.BlockSpec(memory_space=pltpu.VMEM)
-    return pl.pallas_call(
+    out, next_state = pl.pallas_call(
         kernel,
         out_shape=(
             jax.ShapeDtypeStruct(tokens.shape, tokens.dtype),
@@ -467,15 +490,18 @@
             pltpu.VMEM((4, 64, 256), BF16),
             pltpu.VMEM((8, 64, 256), BF16),
             pltpu.VMEM((32, 24, 128), BF16),
-            pltpu.VMEM((8, 2, 256), F32),
+            pltpu.VMEM((8, 2, 128), F32),
+            pltpu.VMEM((8, 2, 128), F32),
             pltpu.VMEM((32, 24, 128), BF16),
             pltpu.VMEM((32, 24, 128), BF16),
             pltpu.VMEM((24, 128), BF16),
             pltpu.VMEM((32, 24, 128), BF16),
             pltpu.VMEM((32, 24, 128), BF16),
-            pltpu.VMEM((8, 2, 256), F32),
+            pltpu.VMEM((8, 2, 128), F32),
+            pltpu.VMEM((8, 2, 128), F32),
             pltpu.VMEM((8, 2, 24, 256), BF16),
             pltpu.VMEM((8, 2, 24, 256), BF16),
+            pltpu.VMEM((2, 24, 256), BF16),
             pltpu.VMEM((8, 2, 24, 256), BF16),
             pltpu.VMEM((32, 24, 128), BF16),
             pltpu.VMEM((32, 24, 128), BF16),
@@ -483,6 +509,9 @@
             pltpu.SemaphoreType.DMA((13,)),
             pltpu.SemaphoreType.DMA((14,)),
             pltpu.SemaphoreType.DMA((14,)),
+            pltpu.SemaphoreType.DMA((8,)),
+            pltpu.SemaphoreType.DMA((8,)),
+            pltpu.SemaphoreType.DMA((8,)),
             pltpu.SemaphoreType.REGULAR,
         ],
         compiler_params=pltpu.CompilerParams(collective_id=0, has_side_effects=True, vmem_limit_bytes=16 * 1024 * 1024),
@@ -502,6 +531,18 @@
         w_up,
         w_down.T,
     )))
+    return pl.pallas_call(
+        place,
+        out_shape=(
+            jax.ShapeDtypeStruct(out.shape, out.dtype),
+            jax.ShapeDtypeStruct(next_state.shape, next_state.dtype),
+        ),
+        in_specs=[vmem_spec, vmem_spec],
+        out_specs=(any_spec, any_spec),
+        scratch_shapes=[pltpu.SemaphoreType.DMA((7,))],
+        compiler_params=pltpu.CompilerParams(vmem_limit_bytes=4 * 1024 * 1024),
+        name="place_outputs",
+    )(out, next_state)
 
 
 def solution(mesh):

time: 61.1 us -> 61 us (level)
  local copies, waits for them, and re-layouts: 1.74 us -> 0 us
  Pallas kernels: 58.6 us -> 59.8 us
    unnamed x2 -> x0, local copies, waits for them, and re-layouts: 1.74 us -> none
    pallas_call x0 -> x1, Pallas kernels: none -> 1.2 us  [body(): pl.pallas_call(place, out_shape=(jax.ShapeDtypeStruct(out.shape, out.dtyp...]
where the time goes in v4:
time: 61 us; the launch traced here: 60.5 us
  Pallas kernels  59.8 us (98%)
  between operations  0.64 us (1%)
    pallas_call x1, Pallas kernels, body(): pl.pallas_call(kernel, out_shape=(jax.ShapeDtypeStruct(tokens.shape, toke...  58.6 us

profile of v4, /device:TPU:1, one launch (start us, length us, event | category | flops | bytes accessed | tf_op | source)
XLA Modules:
  0.0 60.5 jit_solution(1791590613342526446)
XLA Ops:
  0.6 58.6 %decode_layer.1 = (bf16[48,64]{1,0:T(8,128)(2,1)S(1)}, f32[12,2,128,128]{3,2,1,0:T(8,128)S(1)}) custom-call(bf16[48,64]{1,0:T(8,128)(2,1)} %tokens_hbm.1, f32[1,64]{1,0:T(1,128)} %bitcast.8, f32[1,64]{1,0:T(1,128)} %bitcast.9, bf16[64,256]{1,0:T(8,128)(2,1)} %wq_hbm.1, bf16[64,256]{1,0:T(8,128)(2,1)} %wf_hbm.1, bf16[64,256]{1,0:T(8,128)(2,1)} %wi_hbm.1, ...), custom_call_target="tpu_custom_call" | custom-call | tf_op jit(solution)/shard_map/decode_layer/pallas_call | solution.py:469
  59.3 1.2 %place_outputs.1 = (bf16[48,64]{1,0:T(8,128)(2,1)}, f32[12,2,128,128]{3,2,1,0:T(8,128)}) custom-call(bf16[48,64]{1,0:T(8,128)(2,1)S(1)} %get-tuple-element.4.out_v, f32[12,2,128,128]{3,2,1,0:T(8,128)S(1)} %get-tuple-element.5.next_v), custom_call_target="tpu_custom_call" | custom-call | tf_op jit(solution)/shard_map/place_outputs/pallas_call | solution.py:534

commit v5 on v3

--- a/solution.py
+++ b/solution.py
@@ -30,6 +30,7 @@
 ALONG_X = by_distance((4,))
 ALONG_Y = by_distance((4, 2))
 ALONG_Z = by_distance((8,))
+NEAR_Z = [0, 1, 7, 2, 6, 3, 5, 4]
 
 
 def wait_for(ref, sem):
@@ -129,6 +130,7 @@
     in_sems,
     send_sems,
     recv_sems,
+    hidden_sems,
     far_sem,
 ):
     kv, t = lax.axis_index("kv"), lax.axis_index("tp")
@@ -144,12 +146,12 @@
     kvs = [[pz * NX + px for px in xs] for pz in zs]
     ts = [[2 * py + pc for pc in cores] for py in ys]
 
-    def copy_to(src, dst, k, pkv, pt):
+    def copy_to(src, dst, k, pkv, pt, arrived=None):
         return pltpu.make_async_remote_copy(
             src_ref=src,
             dst_ref=dst,
             send_sem=send_sems.at[k],
-            recv_sem=recv_sems.at[k],
+            recv_sem=recv_sems.at[k] if arrived is None else arrived,
             device_id=(pkv, pt),
             device_id_type=MESH,
         )
@@ -220,10 +222,11 @@
 
     for (dx,) in ALONG_X:
         copy_to(gains.at[x], gains.at[x], 1, kvs[0][dx], t).start()
-        copy_to(w4_v.at[xs[dx]], w_first.at[x], 2, kvs[0][dx], t).start()
     own_tok = tok_all.at[x * NT + t]
     for dx, dy, dc in PLANE:
         copy_to(own_tok, own_tok, 0, kvs[0][dx], ts[dy][dc]).start()
+    for (dx,) in ALONG_X:
+        copy_to(w4_v.at[xs[dx]], w_first.at[x], 2, kvs[0][dx], t).start()
     leaving.append((tok_all.at[pl.ds(0, 31)], 0))
     leaving.append((gains.at[pl.ds(0, 3)], 1))
     leaving.append((w_first.at[pl.ds(0, 3)], 2))
@@ -367,8 +370,8 @@
             up_out[pz, half] = partial2[at : at + 24].astype(BF16)
 
     for (dz,) in ALONG_Z:
+        copy_to(up_out.at[zs[dz]], up_in.at[z], 11, kvs[dz][0], t).start()
         copy_to(sq2.at[z], sq2.at[z], 10, kvs[dz][0], t).start()
-        copy_to(up_out.at[zs[dz]], up_in.at[z], 11, kvs[dz][0], t).start()
     up_in[z] = up_out[z]
     leaving.append((sq2.at[pl.ds(0, 7)], 10))
     leaving.append((up_in.at[pl.ds(0, 7)], 11))
@@ -389,31 +392,38 @@
         total = jnp.maximum(total * scales[half], 0.0)
         hidden_all[z, half] = (total * total).astype(BF16)
 
+    own_hidden = hidden_all.at[z]
     for (dz,) in ALONG_Z:
-        copy_to(hidden_all.at[z], hidden_all.at[z], 12, kvs[dz][0], t).start()
+        copy_to(own_hidden, own_hidden, 12, kvs[dz][0], t, hidden_sems.at[z]).start()
     leaving.append((hidden_all.at[pl.ds(0, 7)], 12))
     wait_for(w_down.at[pl.ds(0, 3)], recv_sems.at[7])
-    wait_for(hidden_all.at[pl.ds(0, 7)], recv_sems.at[12])
-
-    partial3 = dot_t(hidden_all[...].reshape(384, 256), w_down[...].reshape(256, 256))
-    for pt in range(NT):
+
+    down_at = t * NX + x
+    for dz in NEAR_Z:
+        pt = zs[dz]
+        if dz:
+            wait_for(hidden_all.at[pt], hidden_sems.at[pt])
+        partial = dot_t(hidden_all[pt].reshape(48, 256), w_down[...].reshape(256, 256))
         for pair in range(2):
-            upper = partial3[48 * pt : 48 * pt + 24, 128 * pair : 128 * pair + 128]
-            lower = partial3[48 * pt + 24 : 48 * pt + 48, 128 * pair : 128 * pair + 128]
+            upper = partial[0:24, 128 * pair : 128 * pair + 128]
+            lower = partial[24:48, 128 * pair : 128 * pair + 128]
             down_out[pt * NX + 2 * pair] = jnp.where(low, upper, swap_lanes(lower)).astype(BF16)
             down_out[pt * NX + 2 * pair + 1] = jnp.where(low, swap_lanes(upper), lower).astype(
                 BF16
             )
-
-    for dx, dy, dc in PLANE:
-        copy_to(
-            down_out.at[ts[dy][dc] * NX + xs[dx]],
-            down_in.at[t * NX + x],
-            13,
-            kvs[0][dx],
-            ts[dy][dc],
-        ).start()
-    down_in[t * NX + x] = down_out[t * NX + x]
+        for dx in (2, 1, 3):
+            copy_to(
+                down_out.at[pt * NX + xs[dx]], down_in.at[down_at], 13, kvs[0][dx], pt
+            ).start()
+
+        @pl.when(pt != t)
+        def _():
+            copy_to(down_out.at[pt * NX + x], down_in.at[down_at], 13, kv, pt).start()
+
+        @pl.when(pt == t)
+        def _():
+            down_in[down_at] = down_out[down_at]
+
     leaving.append((down_in.at[pl.ds(0, 31)], 13))
     wait_for(down_in.at[pl.ds(0, 31)], recv_sems.at[13])
     total = down_in[0].astype(F32)
@@ -423,6 +433,20 @@
     out_ref[...] = jnp.concatenate([total[:, 0:64], total[:, 64:128]], axis=0).astype(BF16)
 
     finish()
+
+
+def place(out_v, next_v, out_hbm, next_hbm, sems):
+    copies = [
+        pltpu.make_async_copy(
+            next_v.at[pl.ds(2 * q, 2)], next_hbm.at[pl.ds(2 * q, 2)], sems.at[q]
+        )
+        for q in range(6)
+    ]
+    copies.append(pltpu.make_async_copy(out_v, out_hbm, sems.at[6]))
+    for copy in copies:
+        copy.start()
+    for copy in copies:
+        copy.wait()
 
 
 def body(
@@ -443,7 +467,7 @@
     bound = lower_bound.reshape(2, 128)
     any_spec = pl.BlockSpec(memory_space=pltpu.HBM)
     vmem_spec = pl.BlockSpec(memory_space=pltpu.VMEM)
-    return pl.pallas_call(
+    out, next_state = pl.pallas_call(
         kernel,
         out_shape=(
             jax.ShapeDtypeStruct(tokens.shape, tokens.dtype),
@@ -483,6 +507,7 @@
             pltpu.SemaphoreType.DMA((13,)),
             pltpu.SemaphoreType.DMA((14,)),
             pltpu.SemaphoreType.DMA((14,)),
+            pltpu.SemaphoreType.DMA((8,)),
             pltpu.SemaphoreType.REGULAR,
         ],
         compiler_params=pltpu.CompilerParams(collective_id=0, has_side_effects=True, vmem_limit_bytes=16 * 1024 * 1024),
@@ -502,6 +527,18 @@
         w_up,
         w_down.T,
     )))
+    return pl.pallas_call(
+        place,
+        out_shape=(
+            jax.ShapeDtypeStruct(out.shape, out.dtype),
+            jax.ShapeDtypeStruct(next_state.shape, next_state.dtype),
+        ),
+        in_specs=[vmem_spec, vmem_spec],
+        out_specs=(any_spec, any_spec),
+        scratch_shapes=[pltpu.SemaphoreType.DMA((7,))],
+        compiler_params=pltpu.CompilerParams(vmem_limit_bytes=4 * 1024 * 1024),
+        name="place_outputs",
+    )(out, next_state)
 
 
 def solution(mesh):

time: 61.1 us -> 59.2 us (0.969)
  local copies, waits for them, and re-layouts: 1.74 us -> 0 us
    pallas_call x1, Pallas kernels: 58.6 us -> 56.9 us  [body(): pl.pallas_call(kernel, out_shape=(jax.ShapeDtypeStruct(tokens.shape, toke...]
    unnamed x2 -> x0, local copies, waits for them, and re-layouts: 1.74 us -> none
    pallas_call x0 -> x1, Pallas kernels: none -> 1.2 us  [body(): pl.pallas_call(place, out_shape=(jax.ShapeDtypeStruct(out.shape, out.dtyp...]
where the time goes in v5:
time: 59.2 us; the launch traced here: 58.7 us
  Pallas kernels  58.1 us (98%)
  between operations  0.64 us (1%)
    pallas_call x1, Pallas kernels, body(): pl.pallas_call(kernel, out_shape=(jax.ShapeDtypeStruct(tokens.shape, toke...  56.9 us
    pallas_call x1, Pallas kernels, body(): pl.pallas_call(place, out_shape=(jax.ShapeDtypeStruct(out.shape, out.dtyp...  1.2 us

profile of v5, /device:TPU:1, one launch (start us, length us, event | category | flops | bytes accessed | tf_op | source)
XLA Modules:
  0.0 58.7 jit_solution(1472738850365642668)
XLA Ops:
  0.6 56.9 %decode_layer.1 = (bf16[48,64]{1,0:T(8,128)(2,1)S(1)}, f32[12,2,128,128]{3,2,1,0:T(8,128)S(1)}) custom-call(bf16[48,64]{1,0:T(8,128)(2,1)} %tokens_hbm.1, f32[1,64]{1,0:T(1,128)} %bitcast.8, f32[1,64]{1,0:T(1,128)} %bitcast.9, bf16[64,256]{1,0:T(8,128)(2,1)} %wq_hbm.1, bf16[64,256]{1,0:T(8,128)(2,1)} %wf_hbm.1, bf16[64,256]{1,0:T(8,128)(2,1)} %wi_hbm.1, ...), custom_call_target="tpu_custom_call" | custom-call | tf_op jit(solution)/shard_map/decode_layer/pallas_call | solution.py:470
  57.5 1.2 %place_outputs.1 = (bf16[48,64]{1,0:T(8,128)(2,1)}, f32[12,2,128,128]{3,2,1,0:T(8,128)}) custom-call(bf16[48,64]{1,0:T(8,128)(2,1)S(1)} %get-tuple-element.4.out_v, f32[12,2,128,128]{3,2,1,0:T(8,128)S(1)} %get-tuple-element.5.next_v), custom_call_target="tpu_custom_call" | custom-call | tf_op jit(solution)/shard_map/place_outputs/pallas_call | solution.py:530

commit v6 on v5

--- a/solution.py
+++ b/solution.py
@@ -29,6 +29,7 @@
 COLUMN = by_distance((8, 4))
 ALONG_X = by_distance((4,))
 ALONG_Y = by_distance((4, 2))
+ROW = by_distance((4, 2))
 ALONG_Z = by_distance((8,))
 NEAR_Z = [0, 1, 7, 2, 6, 3, 5, 4]
 
@@ -63,7 +64,8 @@
     total = pieces[0] * pieces[0]
     for p in pieces[1:]:
         total = total + p * p
-    total = jnp.concatenate([total, jnp.zeros((64, 128), F32)], axis=0)
+    spare = -total.shape[0] % 128
+    total = jnp.concatenate([total, jnp.zeros((spare, 128), F32)], axis=0)
     high = total.astype(BF16)
     rest = (total - high.astype(F32)).astype(BF16)
     lane = lax.broadcasted_iota(jnp.int32, (8, 128), 1)
@@ -75,9 +77,10 @@
     return sums[0:2, :]
 
 
-def column_of(values, base, period):
-    lane = lax.broadcasted_iota(jnp.int32, (24, 256), 1)
-    row = lax.broadcasted_iota(jnp.int32, (24, 256), 0)
+def column_of(values, base, period, rows=24):
+    shape = (rows, values.shape[1])
+    lane = lax.broadcasted_iota(jnp.int32, shape, 1)
+    row = lax.broadcasted_iota(jnp.int32, shape, 0)
     return jnp.sum(
         jnp.where(lane == base + row % period, values, 0.0), axis=1, keepdims=True
     )
@@ -136,8 +139,7 @@
     kv, t = lax.axis_index("kv"), lax.axis_index("tp")
     z, x = kv // NX, kv % NX
     y, core = t // 2, t % 2
-    rows_at = (t + NZ - z) % NZ
-    has_self = t == (2 * z) % NZ
+    has_self = t == z
 
     xs = [(x + d) % 4 for d in range(4)]
     ys = [(y + d) % 4 for d in range(4)]
@@ -210,9 +212,9 @@
     for k in range(2, 9):
         loads[k].wait()
     w_first[x] = w4_v[x]
-    w_up[x] = wup_v[:, pl.ds(pl.multiple_of(x * 256, 256), 256)]
+    w_up[y, x] = wup_v[:, pl.ds(pl.multiple_of(x * 256, 256), 256)]
     w_out[t] = wout_v[...]
-    w_down[x] = wdown_v[:, pl.ds(pl.multiple_of(x * 256, 256), 256)]
+    w_down[y, x] = wdown_v[:, pl.ds(pl.multiple_of(x * 256, 256), 256)]
 
     pl.semaphore_wait(barrier, 31 + 16)
     for step in (2, 6):
@@ -237,6 +239,13 @@
         copy_to(w_out.at[t], w_out.at[t], 3, kv, ts[dy][dc]).start()
     leaving.append((w_out.at[pl.ds(0, 7)], 3))
 
+    for (dx,) in ALONG_X:
+        cols = pl.ds(pl.multiple_of(xs[dx] * 256, 256), 256)
+        copy_to(wup_v.at[:, cols], w_up.at[y, x], 6, kvs[0][dx], t).start()
+        copy_to(wdown_v.at[:, cols], w_down.at[y, x], 7, kvs[0][dx], t).start()
+    leaving.append((w_first.at[pl.ds(0, 3)], 6))
+    leaving.append((w_first.at[pl.ds(0, 3)], 7))
+
     raw = [
         tok_all[pl.ds(NT * q, NT)].astype(F32).reshape(192, 128) for q in range(NX)
     ]
@@ -267,12 +276,10 @@
     leaving.append((sq1.at[pl.ds(0, 7)], 4))
     leaving.append((proj_in.at[pl.ds(0, 31)], 5))
 
-    for (dx,) in ALONG_X:
-        cols = pl.ds(pl.multiple_of(xs[dx] * 256, 256), 256)
-        copy_to(wup_v.at[:, cols], w_up.at[x], 6, kvs[0][dx], t).start()
-        copy_to(wdown_v.at[:, cols], w_down.at[x], 7, kvs[0][dx], t).start()
-    leaving.append((w_up.at[pl.ds(0, 3)], 6))
-    leaving.append((w_down.at[pl.ds(0, 3)], 7))
+    wait_for(w_first.at[pl.ds(0, 3)], recv_sems.at[6])
+    for (dy,) in ALONG_X:
+        copy_to(w_up.at[y], w_up.at[y], 14, kv, ts[dy][0]).start()
+    leaving.append((w_up.at[pl.ds(0, 3)], 14))
 
     for k in range(9, 12):
         loads[k].wait()
@@ -311,11 +318,11 @@
 
     mix_at = t * NX + x
     for dz, dx in COLUMN:
-        copy_to(mix_own, mix_all.at[mix_at], 8, kvs[dz][dx], (z + zs[dz]) % NZ).start()
+        copy_to(mix_own, mix_all.at[mix_at], 8, kvs[dz][dx], z).start()
 
     @pl.when(jnp.logical_not(has_self))
     def _():
-        copy_to(mix_own, mix_all.at[mix_at], 8, kv, (2 * z) % NZ).start()
+        copy_to(mix_own, mix_all.at[mix_at], 8, kv, z).start()
 
     @pl.when(has_self)
     def _():
@@ -349,26 +356,27 @@
     top = jnp.where(low, folded[0], swap_lanes(folded[2]))
     bottom = jnp.where(low, swap_lanes(folded[1]), folded[3])
     attn = jnp.where(head0, top, bottom)
-    own_at = x * NT + rows_at
-    mixed_all[own_at] = (tok_all[own_at].astype(F32) + attn).astype(BF16)
-
-    for dx, dy, dc in PLANE:
-        copy_to(mixed_all.at[own_at], mixed_all.at[own_at], 9, kvs[0][dx], ts[dy][dc]).start()
-    leaving.append((mixed_all.at[pl.ds(0, 31)], 9))
-    wait_for(w_up.at[pl.ds(0, 3)], recv_sems.at[6])
-    wait_for(mixed_all.at[pl.ds(0, 31)], recv_sems.at[9])
-
-    raw2 = [
-        mixed_all[pl.ds(NT * q, NT)].astype(F32).reshape(192, 128) for q in range(NX)
-    ]
+    own_at = 2 * x + core
+    mixed_all[own_at] = (tok_all[x * NT + t].astype(F32) + attn).astype(BF16)
+
+    own_mixed = mixed_all.at[own_at]
+    for dx, dc in ROW:
+        copy_to(own_mixed, own_mixed, 9, kvs[0][dx], ts[0][dc]).start()
+    leaving.append((mixed_all.at[pl.ds(0, 7)], 9))
+
+    wait_for(w_first.at[pl.ds(0, 3)], recv_sems.at[7])
+    for (dy,) in ALONG_X:
+        copy_to(w_down.at[y], w_down.at[y], 15, kv, ts[dy][0]).start()
+    leaving.append((w_down.at[pl.ds(0, 3)], 15))
+    wait_for(w_up.at[pl.ds(0, 3)], recv_sems.at[14])
+    wait_for(mixed_all.at[pl.ds(0, 7)], recv_sems.at[9])
+    raw2 = [mixed_all[2 * q : 2 * q + 2].astype(F32).reshape(48, 128) for q in range(NX)]
     sq2[z] = row_squares(raw2)
     lhs2 = unpacked([raw2[q] * gains[q, 1:2, :] for q in range(NX)])
-    partial2 = jnp.dot(lhs2, w_up[...].reshape(256, 256), preferred_element_type=F32)
-    for half in range(2):
-        for pz in range(NZ):
-            at = half * 192 + pz * 24
-            up_out[pz, half] = partial2[at : at + 24].astype(BF16)
-
+    for q in range(4):
+        partial2 = jnp.dot(lhs2, w_up[q].reshape(256, 256), preferred_element_type=F32)
+        up_out[2 * q] = partial2[:, 0:128].astype(BF16)
+        up_out[2 * q + 1] = partial2[:, 128:256].astype(BF16)
     for (dz,) in ALONG_Z:
         copy_to(up_out.at[zs[dz]], up_in.at[z], 11, kvs[dz][0], t).start()
         copy_to(sq2.at[z], sq2.at[z], 10, kvs[dz][0], t).start()
@@ -379,57 +387,50 @@
     squares2 = sq2[0]
     for q in range(1, NZ):
         squares2 = squares2 + sq2[q]
-    scales = [
-        lax.rsqrt(column_of(squares2[q : q + 1, :], z * 24, 24) / WIDTH + NORM_EPS)
-        for q in range(2)
-    ]
+    scale2 = jnp.concatenate(
+        [
+            lax.rsqrt(column_of(squares2[q : q + 1, :], 0, 48, 48) / WIDTH + NORM_EPS)
+            for q in range(2)
+        ],
+        axis=0,
+    )
     wait_for(up_in.at[pl.ds(0, 7)], recv_sems.at[11])
 
-    for half in range(2):
-        total = up_in[0, half].astype(F32)
-        for q in range(1, NZ):
-            total = total + up_in[q, half].astype(F32)
-        total = jnp.maximum(total * scales[half], 0.0)
-        hidden_all[z, half] = (total * total).astype(BF16)
-
+    total = up_in[0].astype(F32)
+    for q in range(1, NZ):
+        total = total + up_in[q].astype(F32)
+    total = jnp.maximum(total * scale2, 0.0)
+    hidden_all[z] = (total * total).astype(BF16)
     own_hidden = hidden_all.at[z]
     for (dz,) in ALONG_Z:
         copy_to(own_hidden, own_hidden, 12, kvs[dz][0], t, hidden_sems.at[z]).start()
     leaving.append((hidden_all.at[pl.ds(0, 7)], 12))
-    wait_for(w_down.at[pl.ds(0, 3)], recv_sems.at[7])
-
-    down_at = t * NX + x
+    wait_for(w_down.at[pl.ds(0, 3)], recv_sems.at[15])
+
+    partial3 = jnp.zeros((96, 256), F32)
     for dz in NEAR_Z:
-        pt = zs[dz]
+        pz = zs[dz]
         if dz:
-            wait_for(hidden_all.at[pt], hidden_sems.at[pt])
-        partial = dot_t(hidden_all[pt].reshape(48, 256), w_down[...].reshape(256, 256))
+            wait_for(hidden_all.at[pz], hidden_sems.at[pz])
+        units = pl.ds(pl.multiple_of((pz % 2) * 128, 128), 128)
+        partial3 = partial3 + dot_t(hidden_all[pz], w_down[pz // 2, :, :, units].reshape(256, 128))
+    for half in range(2):
         for pair in range(2):
-            upper = partial[0:24, 128 * pair : 128 * pair + 128]
-            lower = partial[24:48, 128 * pair : 128 * pair + 128]
-            down_out[pt * NX + 2 * pair] = jnp.where(low, upper, swap_lanes(lower)).astype(BF16)
-            down_out[pt * NX + 2 * pair + 1] = jnp.where(low, swap_lanes(upper), lower).astype(
-                BF16
-            )
-        for dx in (2, 1, 3):
-            copy_to(
-                down_out.at[pt * NX + xs[dx]], down_in.at[down_at], 13, kvs[0][dx], pt
-            ).start()
-
-        @pl.when(pt != t)
-        def _():
-            copy_to(down_out.at[pt * NX + x], down_in.at[down_at], 13, kv, pt).start()
-
-        @pl.when(pt == t)
-        def _():
-            down_in[down_at] = down_out[down_at]
-
-    leaving.append((down_in.at[pl.ds(0, 31)], 13))
-    wait_for(down_in.at[pl.ds(0, 31)], recv_sems.at[13])
+            upper = partial3[24 * half : 24 * half + 24, 128 * pair : 128 * pair + 128]
+            lower = partial3[48 + 24 * half : 72 + 24 * half, 128 * pair : 128 * pair + 128]
+            down_out[4 * pair + half] = jnp.where(low, upper, swap_lanes(lower)).astype(BF16)
+            down_out[4 * pair + 2 + half] = jnp.where(low, swap_lanes(upper), lower).astype(BF16)
+    for dx, dc in ROW:
+        copy_to(
+            down_out.at[2 * xs[dx] + cores[dc]], down_in.at[own_at], 13, kvs[0][dx], ts[0][dc]
+        ).start()
+    down_in[own_at] = down_out[own_at]
+    leaving.append((down_in.at[pl.ds(0, 7)], 13))
+    wait_for(down_in.at[pl.ds(0, 7)], recv_sems.at[13])
     total = down_in[0].astype(F32)
-    for q in range(1, 32):
+    for q in range(1, 8):
         total = total + down_in[q].astype(F32)
-    total = mixed_all[x * NT + t].astype(F32) + total
+    total = mixed_all[own_at].astype(F32) + total
     out_ref[...] = jnp.concatenate([total[:, 0:64], total[:, 64:128]], axis=0).astype(BF16)
 
     finish()
@@ -487,8 +488,8 @@
             pltpu.VMEM((64, 1024), BF16),
             pltpu.VMEM((4, 2, 128), F32),
             pltpu.VMEM((4, 64, 256), BF16),
-            pltpu.VMEM((4, 64, 256), BF16),
-            pltpu.VMEM((4, 64, 256), BF16),
+            pltpu.VMEM((4, 4, 64, 256), BF16),
+            pltpu.VMEM((4, 4, 64, 256), BF16),
             pltpu.VMEM((8, 64, 256), BF16),
             pltpu.VMEM((32, 24, 128), BF16),
             pltpu.VMEM((8, 2, 256), F32),
@@ -496,17 +497,17 @@
             pltpu.VMEM((32, 24, 128), BF16),
             pltpu.VMEM((24, 128), BF16),
             pltpu.VMEM((32, 24, 128), BF16),
-            pltpu.VMEM((32, 24, 128), BF16),
-            pltpu.VMEM((8, 2, 256), F32),
-            pltpu.VMEM((8, 2, 24, 256), BF16),
-            pltpu.VMEM((8, 2, 24, 256), BF16),
-            pltpu.VMEM((8, 2, 24, 256), BF16),
-            pltpu.VMEM((32, 24, 128), BF16),
-            pltpu.VMEM((32, 24, 128), BF16),
+            pltpu.VMEM((8, 24, 128), BF16),
+            pltpu.VMEM((8, 2, 128), F32),
+            pltpu.VMEM((8, 96, 128), BF16),
+            pltpu.VMEM((8, 96, 128), BF16),
+            pltpu.VMEM((8, 96, 128), BF16),
+            pltpu.VMEM((8, 24, 128), BF16),
+            pltpu.VMEM((8, 24, 128), BF16),
             pltpu.VMEM((24, 128), F32),
             pltpu.SemaphoreType.DMA((13,)),
-            pltpu.SemaphoreType.DMA((14,)),
-            pltpu.SemaphoreType.DMA((14,)),
+            pltpu.SemaphoreType.DMA((16,)),
+            pltpu.SemaphoreType.DMA((16,)),
             pltpu.SemaphoreType.DMA((8,)),
             pltpu.SemaphoreType.REGULAR,
         ],

time: 59.2 us -> 56.4 us (0.953)
  Pallas kernels: 58.1 us -> 55.6 us
    pallas_call x1, Pallas kernels: 56.9 us -> 54.4 us  [body(): pl.pallas_call(kernel, out_shape=(jax.ShapeDtypeStruct(tokens.shape, toke...]
where the time goes in v6:
time: 56.4 us; the launch traced here: 56.2 us
  Pallas kernels  55.6 us (99%)
  between operations  0.64 us (1%)
    pallas_call x1, Pallas kernels, body(): pl.pallas_call(kernel, out_shape=(jax.ShapeDtypeStruct(tokens.shape, toke...  54.4 us
    pallas_call x1, Pallas kernels, body(): pl.pallas_call(place, out_shape=(jax.ShapeDtypeStruct(out.shape, out.dtyp...  1.2 us

profile of v6, /device:TPU:1, one launch (start us, length us, event | category | flops | bytes accessed | tf_op | source)
XLA Modules:
  0.0 56.2 jit_solution(6560559287517744831)
XLA Ops:
  0.6 54.4 %decode_layer.1 = (bf16[48,64]{1,0:T(8,128)(2,1)S(1)}, f32[12,2,128,128]{3,2,1,0:T(8,128)S(1)}) custom-call(bf16[48,64]{1,0:T(8,128)(2,1)} %tokens_hbm.1, f32[1,64]{1,0:T(1,128)} %bitcast.8, f32[1,64]{1,0:T(1,128)} %bitcast.9, bf16[64,256]{1,0:T(8,128)(2,1)} %wq_hbm.1, bf16[64,256]{1,0:T(8,128)(2,1)} %wf_hbm.1, bf16[64,256]{1,0:T(8,128)(2,1)} %wi_hbm.1, ...), custom_call_target="tpu_custom_call" | custom-call | tf_op jit(solution)/shard_map/decode_layer/pallas_call | solution.py:471
  55.0 1.2 %place_outputs.1 = (bf16[48,64]{1,0:T(8,128)(2,1)}, f32[12,2,128,128]{3,2,1,0:T(8,128)}) custom-call(bf16[48,64]{1,0:T(8,128)(2,1)S(1)} %get-tuple-element.4.out_v, f32[12,2,128,128]{3,2,1,0:T(8,128)S(1)} %get-tuple-element.5.next_v), custom_call_target="tpu_custom_call" | custom-call | tf_op jit(solution)/shard_map/place_outputs/pallas_call | solution.py:531

commit v7 on v6

--- a/solution.py
+++ b/solution.py
@@ -29,7 +29,8 @@
 COLUMN = by_distance((8, 4))
 ALONG_X = by_distance((4,))
 ALONG_Y = by_distance((4, 2))
-ROW = by_distance((4, 2))
+PAIR = by_distance((2, 4))
+ROW = by_distance((2, 4, 2))
 ALONG_Z = by_distance((8,))
 NEAR_Z = [0, 1, 7, 2, 6, 3, 5, 4]
 
@@ -53,8 +54,8 @@
 def unpacked(pieces):
     low = low_lanes(pieces[0].shape)
     swapped = [swap_lanes(p) for p in pieces]
-    first = [jnp.where(low, pieces[i], swapped[i + 1]).astype(BF16) for i in (0, 2)]
-    second = [jnp.where(low, swapped[i], pieces[i + 1]).astype(BF16) for i in (0, 2)]
+    first = [jnp.where(low, pieces[i], swapped[i + 1]).astype(BF16) for i in range(0, len(pieces), 2)]
+    second = [jnp.where(low, swapped[i], pieces[i + 1]).astype(BF16) for i in range(0, len(pieces), 2)]
     return jnp.concatenate(
         [jnp.concatenate(first, axis=1), jnp.concatenate(second, axis=1)], axis=0
     )
@@ -172,6 +173,11 @@
             def _():
                 wait_for(mix_all, send_sems.at[8])
 
+    pair, odd = z // 2, z % 2
+    pair_kvs = [kvs[0], [(z + 1 - 2 * odd) * NX + px for px in xs]]
+    pair_odd = [odd, 1 - odd]
+    in_pair = odd * NX + x
+
     barrier = pltpu.get_barrier_semaphore()
 
     def tell(pkv, pt):
@@ -201,6 +207,9 @@
     for load in loads:
         load.start()
 
+    def units_of(px, p):
+        return pl.ds(pl.multiple_of(px * 256 + p * 128, 128), 128)
+
     loads[0].wait()
     tok_f = tok_v[...].astype(F32)
     tok_all[x * NT + t] = jnp.concatenate([tok_f[0:24], tok_f[24:48]], axis=1).astype(BF16)
@@ -208,13 +217,13 @@
     loads[12].wait()
     for q in range(2):
         g = gain_v[q]
-        gains[x, q : q + 1, :] = jnp.concatenate([g, g], axis=1)
+        gains[in_pair, q : q + 1, :] = jnp.concatenate([g, g], axis=1)
     for k in range(2, 9):
         loads[k].wait()
     w_first[x] = w4_v[x]
-    w_up[y, x] = wup_v[:, pl.ds(pl.multiple_of(x * 256, 256), 256)]
+    w_up[y, in_pair] = wup_v[:, units_of(x, odd)]
     w_out[t] = wout_v[...]
-    w_down[y, x] = wdown_v[:, pl.ds(pl.multiple_of(x * 256, 256), 256)]
+    w_down[y, in_pair] = wdown_v[:, units_of(x, odd)]
 
     pl.semaphore_wait(barrier, 31 + 16)
     for step in (2, 6):
@@ -222,35 +231,35 @@
             far_sem, inc=1, device_id=(kvs[step][0], t), device_id_type=MESH
         )
 
-    for (dx,) in ALONG_X:
-        copy_to(gains.at[x], gains.at[x], 1, kvs[0][dx], t).start()
+    for dp, dx in PAIR:
+        copy_to(gains.at[in_pair], gains.at[in_pair], 1, pair_kvs[dp][dx], t).start()
     own_tok = tok_all.at[x * NT + t]
     for dx, dy, dc in PLANE:
         copy_to(own_tok, own_tok, 0, kvs[0][dx], ts[dy][dc]).start()
     for (dx,) in ALONG_X:
         copy_to(w4_v.at[xs[dx]], w_first.at[x], 2, kvs[0][dx], t).start()
     leaving.append((tok_all.at[pl.ds(0, 31)], 0))
-    leaving.append((gains.at[pl.ds(0, 3)], 1))
+    leaving.append((gains.at[pl.ds(0, 7)], 1))
     leaving.append((w_first.at[pl.ds(0, 3)], 2))
-    wait_for(gains.at[pl.ds(0, 3)], recv_sems.at[1])
+    wait_for(gains.at[pl.ds(0, 7)], recv_sems.at[1])
     wait_for(tok_all.at[pl.ds(0, 31)], recv_sems.at[0])
 
     for dy, dc in ALONG_Y:
         copy_to(w_out.at[t], w_out.at[t], 3, kv, ts[dy][dc]).start()
     leaving.append((w_out.at[pl.ds(0, 7)], 3))
 
-    for (dx,) in ALONG_X:
-        cols = pl.ds(pl.multiple_of(xs[dx] * 256, 256), 256)
-        copy_to(wup_v.at[:, cols], w_up.at[y, x], 6, kvs[0][dx], t).start()
-        copy_to(wdown_v.at[:, cols], w_down.at[y, x], 7, kvs[0][dx], t).start()
-    leaving.append((w_first.at[pl.ds(0, 3)], 6))
-    leaving.append((w_first.at[pl.ds(0, 3)], 7))
+    for dp, dx in PAIR:
+        cols = units_of(xs[dx], pair_odd[dp])
+        copy_to(wup_v.at[:, cols], w_up.at[y, in_pair], 6, pair_kvs[dp][dx], t).start()
+        copy_to(wdown_v.at[:, cols], w_down.at[y, in_pair], 7, pair_kvs[dp][dx], t).start()
+    leaving.append((w_up.at[0, pl.ds(0, 7)], 6))
+    leaving.append((w_up.at[0, pl.ds(0, 7)], 7))
 
     raw = [
         tok_all[pl.ds(NT * q, NT)].astype(F32).reshape(192, 128) for q in range(NX)
     ]
     sq1[z] = row_squares(raw)
-    lhs = unpacked([raw[q] * gains[q, 0:1, :] for q in range(NX)])
+    lhs = unpacked([raw[q] * gains[odd * NX + q, 0:1, :] for q in range(NX)])
     wait_for(w_first.at[pl.ds(0, 3)], recv_sems.at[2])
     partial = jnp.dot(lhs, w_first[...].reshape(256, 256), preferred_element_type=F32)
 
@@ -276,7 +285,7 @@
     leaving.append((sq1.at[pl.ds(0, 7)], 4))
     leaving.append((proj_in.at[pl.ds(0, 31)], 5))
 
-    wait_for(w_first.at[pl.ds(0, 3)], recv_sems.at[6])
+    wait_for(w_up.at[0, pl.ds(0, 7)], recv_sems.at[6])
     for (dy,) in ALONG_X:
         copy_to(w_up.at[y], w_up.at[y], 14, kv, ts[dy][0]).start()
     leaving.append((w_up.at[pl.ds(0, 3)], 14))
@@ -356,37 +365,35 @@
     top = jnp.where(low, folded[0], swap_lanes(folded[2]))
     bottom = jnp.where(low, swap_lanes(folded[1]), folded[3])
     attn = jnp.where(head0, top, bottom)
-    own_at = 2 * x + core
+    own_at = 2 * in_pair + core
     mixed_all[own_at] = (tok_all[x * NT + t].astype(F32) + attn).astype(BF16)
 
     own_mixed = mixed_all.at[own_at]
-    for dx, dc in ROW:
-        copy_to(own_mixed, own_mixed, 9, kvs[0][dx], ts[0][dc]).start()
-    leaving.append((mixed_all.at[pl.ds(0, 7)], 9))
-
-    wait_for(w_first.at[pl.ds(0, 3)], recv_sems.at[7])
+    for dp, dx, dc in ROW:
+        copy_to(own_mixed, own_mixed, 9, pair_kvs[dp][dx], ts[0][dc]).start()
+    leaving.append((mixed_all.at[pl.ds(0, 15)], 9))
+
+    wait_for(w_up.at[0, pl.ds(0, 7)], recv_sems.at[7])
     for (dy,) in ALONG_X:
         copy_to(w_down.at[y], w_down.at[y], 15, kv, ts[dy][0]).start()
     leaving.append((w_down.at[pl.ds(0, 3)], 15))
     wait_for(w_up.at[pl.ds(0, 3)], recv_sems.at[14])
-    wait_for(mixed_all.at[pl.ds(0, 7)], recv_sems.at[9])
-    raw2 = [mixed_all[2 * q : 2 * q + 2].astype(F32).reshape(48, 128) for q in range(NX)]
-    sq2[z] = row_squares(raw2)
-    lhs2 = unpacked([raw2[q] * gains[q, 1:2, :] for q in range(NX)])
+    wait_for(mixed_all.at[pl.ds(0, 15)], recv_sems.at[9])
+    raw2 = [mixed_all[2 * q : 2 * q + 2].astype(F32).reshape(48, 128) for q in range(8)]
+    sq2[pair] = row_squares(raw2)
+    lhs2 = unpacked([raw2[q] * gains[q, 1:2, :] for q in range(8)])
     for q in range(4):
-        partial2 = jnp.dot(lhs2, w_up[q].reshape(256, 256), preferred_element_type=F32)
-        up_out[2 * q] = partial2[:, 0:128].astype(BF16)
-        up_out[2 * q + 1] = partial2[:, 128:256].astype(BF16)
-    for (dz,) in ALONG_Z:
-        copy_to(up_out.at[zs[dz]], up_in.at[z], 11, kvs[dz][0], t).start()
-        copy_to(sq2.at[z], sq2.at[z], 10, kvs[dz][0], t).start()
-    up_in[z] = up_out[z]
-    leaving.append((sq2.at[pl.ds(0, 7)], 10))
-    leaving.append((up_in.at[pl.ds(0, 7)], 11))
-    wait_for(sq2.at[pl.ds(0, 7)], recv_sems.at[10])
-    squares2 = sq2[0]
-    for q in range(1, NZ):
-        squares2 = squares2 + sq2[q]
+        up_out[q] = jnp.dot(
+            lhs2, w_up[q].reshape(512, 128), preferred_element_type=F32
+        ).astype(BF16)
+    for dz in (4, 2, 6):
+        copy_to(up_out.at[zs[dz] // 2], up_in.at[pair], 11, kvs[dz][0], t).start()
+        copy_to(sq2.at[pair], sq2.at[pair], 10, kvs[dz][0], t).start()
+    up_in[pair] = up_out[pair]
+    leaving.append((sq2.at[pl.ds(0, 3)], 10))
+    leaving.append((up_in.at[pl.ds(0, 3)], 11))
+    wait_for(sq2.at[pl.ds(0, 3)], recv_sems.at[10])
+    squares2 = sq2[0] + sq2[1] + sq2[2] + sq2[3]
     scale2 = jnp.concatenate(
         [
             lax.rsqrt(column_of(squares2[q : q + 1, :], 0, 48, 48) / WIDTH + NORM_EPS)
@@ -394,41 +401,44 @@
         ],
         axis=0,
     )
-    wait_for(up_in.at[pl.ds(0, 7)], recv_sems.at[11])
+    wait_for(up_in.at[pl.ds(0, 3)], recv_sems.at[11])
 
     total = up_in[0].astype(F32)
-    for q in range(1, NZ):
+    for q in range(1, 4):
         total = total + up_in[q].astype(F32)
     total = jnp.maximum(total * scale2, 0.0)
-    hidden_all[z] = (total * total).astype(BF16)
-    own_hidden = hidden_all.at[z]
-    for (dz,) in ALONG_Z:
-        copy_to(own_hidden, own_hidden, 12, kvs[dz][0], t, hidden_sems.at[z]).start()
-    leaving.append((hidden_all.at[pl.ds(0, 7)], 12))
+    hidden_all[pair] = (total * total).astype(BF16)
+    own_hidden = hidden_all.at[pair]
+    for dz in (4, 2, 6):
+        copy_to(own_hidden, own_hidden, 12, kvs[dz][0], t, hidden_sems.at[pair]).start()
+    leaving.append((hidden_all.at[pl.ds(0, 3)], 12))
     wait_for(w_down.at[pl.ds(0, 3)], recv_sems.at[15])
 
-    partial3 = jnp.zeros((96, 256), F32)
-    for dz in NEAR_Z:
-        pz = zs[dz]
+    partial3 = jnp.zeros((96, 512), F32)
+    for dz in (0, 2, 6, 4):
+        pq = zs[dz] // 2
         if dz:
-            wait_for(hidden_all.at[pz], hidden_sems.at[pz])
-        units = pl.ds(pl.multiple_of((pz % 2) * 128, 128), 128)
-        partial3 = partial3 + dot_t(hidden_all[pz], w_down[pz // 2, :, :, units].reshape(256, 128))
+            wait_for(hidden_all.at[pq], hidden_sems.at[pq])
+        partial3 = partial3 + dot_t(hidden_all[pq], w_down[pq].reshape(512, 128))
     for half in range(2):
-        for pair in range(2):
-            upper = partial3[24 * half : 24 * half + 24, 128 * pair : 128 * pair + 128]
-            lower = partial3[48 + 24 * half : 72 + 24 * half, 128 * pair : 128 * pair + 128]
-            down_out[4 * pair + half] = jnp.where(low, upper, swap_lanes(lower)).astype(BF16)
-            down_out[4 * pair + 2 + half] = jnp.where(low, swap_lanes(upper), lower).astype(BF16)
-    for dx, dc in ROW:
+        for two in range(4):
+            upper = partial3[24 * half : 24 * half + 24, 128 * two : 128 * two + 128]
+            lower = partial3[48 + 24 * half : 72 + 24 * half, 128 * two : 128 * two + 128]
+            down_out[4 * two + half] = jnp.where(low, upper, swap_lanes(lower)).astype(BF16)
+            down_out[4 * two + 2 + half] = jnp.where(low, swap_lanes(upper), lower).astype(BF16)
+    for dp, dx, dc in ROW:
         copy_to(
-            down_out.at[2 * xs[dx] + cores[dc]], down_in.at[own_at], 13, kvs[0][dx], ts[0][dc]
+            down_out.at[2 * (pair_odd[dp] * NX + xs[dx]) + cores[dc]],
+            down_in.at[own_at],
+            13,
+            pair_kvs[dp][dx],
+            ts[0][dc],
         ).start()
     down_in[own_at] = down_out[own_at]
-    leaving.append((down_in.at[pl.ds(0, 7)], 13))
-    wait_for(down_in.at[pl.ds(0, 7)], recv_sems.at[13])
+    leaving.append((down_in.at[pl.ds(0, 15)], 13))
+    wait_for(down_in.at[pl.ds(0, 15)], recv_sems.at[13])
     total = down_in[0].astype(F32)
-    for q in range(1, 8):
+    for q in range(1, 16):
         total = total + down_in[q].astype(F32)
     total = mixed_all[own_at].astype(F32) + total
     out_ref[...] = jnp.concatenate([total[:, 0:64], total[:, 64:128]], axis=0).astype(BF16)
@@ -486,10 +496,10 @@
             pltpu.VMEM((64, 256), BF16),
             pltpu.VMEM((64, 1024), BF16),
             pltpu.VMEM((64, 1024), BF16),
-            pltpu.VMEM((4, 2, 128), F32),
+            pltpu.VMEM((8, 2, 128), F32),
             pltpu.VMEM((4, 64, 256), BF16),
-            pltpu.VMEM((4, 4, 64, 256), BF16),
-            pltpu.VMEM((4, 4, 64, 256), BF16),
+            pltpu.VMEM((4, 8, 64, 128), BF16),
+            pltpu.VMEM((4, 8, 64, 128), BF16),
             pltpu.VMEM((8, 64, 256), BF16),
             pltpu.VMEM((32, 24, 128), BF16),
             pltpu.VMEM((8, 2, 256), F32),
@@ -497,13 +507,13 @@
             pltpu.VMEM((32, 24, 128), BF16),
             pltpu.VMEM((24, 128), BF16),
             pltpu.VMEM((32, 24, 128), BF16),
-            pltpu.VMEM((8, 24, 128), BF16),
-            pltpu.VMEM((8, 2, 128), F32),
-            pltpu.VMEM((8, 96, 128), BF16),
-            pltpu.VMEM((8, 96, 128), BF16),
-            pltpu.VMEM((8, 96, 128), BF16),
-            pltpu.VMEM((8, 24, 128), BF16),
-            pltpu.VMEM((8, 24, 128), BF16),
+            pltpu.VMEM((16, 24, 128), BF16),
+            pltpu.VMEM((4, 2, 128), F32),
+            pltpu.VMEM((4, 96, 128), BF16),
+            pltpu.VMEM((4, 96, 128), BF16),
+            pltpu.VMEM((4, 96, 128), BF16),
+            pltpu.VMEM((16, 24, 128), BF16),
+            pltpu.VMEM((16, 24, 128), BF16),
             pltpu.VMEM((24, 128), F32),
             pltpu.SemaphoreType.DMA((13,)),
             pltpu.SemaphoreType.DMA((16,)),

time: 56.4 us -> 56.1 us (level)
  no operation moved by 1% of the time
where the time goes in v7:
time: 56.1 us; the launch traced here: 56 us
  Pallas kernels  55.3 us (99%)
  between operations  0.64 us (1%)
    pallas_call x1, Pallas kernels, body(): pl.pallas_call(kernel, out_shape=(jax.ShapeDtypeStruct(tokens.shape, toke...  54.1 us
    pallas_call x1, Pallas kernels, body(): pl.pallas_call(place, out_shape=(jax.ShapeDtypeStruct(out.shape, out.dtyp...  1.2 us

profile of v7, /device:TPU:1, one launch (start us, length us, event | category | flops | bytes accessed | tf_op | source)
XLA Modules:
  0.0 56.0 jit_solution(5517580589052554244)
XLA Ops:
  0.6 54.1 %decode_layer.1 = (bf16[48,64]{1,0:T(8,128)(2,1)S(1)}, f32[12,2,128,128]{3,2,1,0:T(8,128)S(1)}) custom-call(bf16[48,64]{1,0:T(8,128)(2,1)} %tokens_hbm.1, f32[1,64]{1,0:T(1,128)} %bitcast.8, f32[1,64]{1,0:T(1,128)} %bitcast.9, bf16[64,256]{1,0:T(8,128)(2,1)} %wq_hbm.1, bf16[64,256]{1,0:T(8,128)(2,1)} %wf_hbm.1, bf16[64,256]{1,0:T(8,128)(2,1)} %wi_hbm.1, ...), custom_call_target="tpu_custom_call" | custom-call | tf_op jit(solution)/shard_map/decode_layer/pallas_call | solution.py:481
  54.8 1.2 %place_outputs.1 = (bf16[48,64]{1,0:T(8,128)(2,1)}, f32[12,2,128,128]{3,2,1,0:T(8,128)}) custom-call(bf16[48,64]{1,0:T(8,128)(2,1)S(1)} %get-tuple-element.4.out_v, f32[12,2,128,128]{3,2,1,0:T(8,128)S(1)} %get-tuple-element.5.next_v), custom_call_target="tpu_custom_call" | custom-call | tf_op jit(solution)/shard_map/place_outputs/pallas_call | solution.py:541

commit v8 on v7

--- a/solution.py
+++ b/solution.py
@@ -248,12 +248,6 @@
         copy_to(w_out.at[t], w_out.at[t], 3, kv, ts[dy][dc]).start()
     leaving.append((w_out.at[pl.ds(0, 7)], 3))
 
-    for dp, dx in PAIR:
-        cols = units_of(xs[dx], pair_odd[dp])
-        copy_to(wup_v.at[:, cols], w_up.at[y, in_pair], 6, pair_kvs[dp][dx], t).start()
-        copy_to(wdown_v.at[:, cols], w_down.at[y, in_pair], 7, pair_kvs[dp][dx], t).start()
-    leaving.append((w_up.at[0, pl.ds(0, 7)], 6))
-    leaving.append((w_up.at[0, pl.ds(0, 7)], 7))
 
     raw = [
         tok_all[pl.ds(NT * q, NT)].astype(F32).reshape(192, 128) for q in range(NX)
@@ -284,11 +278,13 @@
     proj_in[kv] = proj_out[kv]
     leaving.append((sq1.at[pl.ds(0, 7)], 4))
     leaving.append((proj_in.at[pl.ds(0, 31)], 5))
-
-    wait_for(w_up.at[0, pl.ds(0, 7)], recv_sems.at[6])
-    for (dy,) in ALONG_X:
-        copy_to(w_up.at[y], w_up.at[y], 14, kv, ts[dy][0]).start()
-    leaving.append((w_up.at[pl.ds(0, 3)], 14))
+    for dp, dx in PAIR:
+        cols = units_of(xs[dx], pair_odd[dp])
+        copy_to(wup_v.at[:, cols], w_up.at[y, in_pair], 6, pair_kvs[dp][dx], t).start()
+        copy_to(wdown_v.at[:, cols], w_down.at[y, in_pair], 7, pair_kvs[dp][dx], t).start()
+    leaving.append((w_up.at[0, pl.ds(0, 7)], 6))
+    leaving.append((w_up.at[0, pl.ds(0, 7)], 7))
+
 
     for k in range(9, 12):
         loads[k].wait()
@@ -337,6 +333,10 @@
     def _():
         mix_all[mix_at] = mix_own[...]
 
+    wait_for(w_up.at[0, pl.ds(0, 7)], recv_sems.at[6])
+    for (dy,) in ALONG_X:
+        copy_to(w_up.at[y], w_up.at[y], 14, kv, ts[dy][0]).start()
+    leaving.append((w_up.at[pl.ds(0, 3)], 14))
     mix_sent.append(1)
     forget_t = jnp.concatenate([forget, pad], axis=0).T
     for j in range(24):

time: 56.1 us -> 54.8 us (0.977)
  Pallas kernels: 55.3 us -> 54 us
    pallas_call x1, Pallas kernels: 54.1 us -> 52.8 us  [body(): pl.pallas_call(kernel, out_shape=(jax.ShapeDtypeStruct(tokens.shape, toke...]
where the time goes in v8:
time: 54.8 us; the launch traced here: 54.7 us
  Pallas kernels  54 us (99%)
  between operations  0.64 us (1%)
    pallas_call x1, Pallas kernels, body(): pl.pallas_call(kernel, out_shape=(jax.ShapeDtypeStruct(tokens.shape, toke...  52.8 us
    pallas_call x1, Pallas kernels, body(): pl.pallas_call(place, out_shape=(jax.ShapeDtypeStruct(out.shape, out.dtyp...  1.2 us

profile of v8, /device:TPU:1, one launch (start us, length us, event | category | flops | bytes accessed | tf_op | source)
XLA Modules:
  0.0 54.7 jit_solution(4413174115062115125)
XLA Ops:
  0.6 52.8 %decode_layer.1 = (bf16[48,64]{1,0:T(8,128)(2,1)S(1)}, f32[12,2,128,128]{3,2,1,0:T(8,128)S(1)}) custom-call(bf16[48,64]{1,0:T(8,128)(2,1)} %tokens_hbm.1, f32[1,64]{1,0:T(1,128)} %bitcast.8, f32[1,64]{1,0:T(1,128)} %bitcast.9, bf16[64,256]{1,0:T(8,128)(2,1)} %wq_hbm.1, bf16[64,256]{1,0:T(8,128)(2,1)} %wf_hbm.1, bf16[64,256]{1,0:T(8,128)(2,1)} %wi_hbm.1, ...), custom_call_target="tpu_custom_call" | custom-call | tf_op jit(solution)/shard_map/decode_layer/pallas_call | solution.py:481
  53.5 1.2 %place_outputs.1 = (bf16[48,64]{1,0:T(8,128)(2,1)}, f32[12,2,128,128]{3,2,1,0:T(8,128)}) custom-call(bf16[48,64]{1,0:T(8,128)(2,1)S(1)} %get-tuple-element.4.out_v, f32[12,2,128,128]{3,2,1,0:T(8,128)S(1)} %get-tuple-element.5.next_v), custom_call_target="tpu_custom_call" | custom-call | tf_op jit(solution)/shard_map/place_outputs/pallas_call | solution.py:541

commit v9 on v8

--- a/solution.py
+++ b/solution.py
@@ -244,10 +244,6 @@
     wait_for(gains.at[pl.ds(0, 7)], recv_sems.at[1])
     wait_for(tok_all.at[pl.ds(0, 31)], recv_sems.at[0])
 
-    for dy, dc in ALONG_Y:
-        copy_to(w_out.at[t], w_out.at[t], 3, kv, ts[dy][dc]).start()
-    leaving.append((w_out.at[pl.ds(0, 7)], 3))
-
 
     raw = [
         tok_all[pl.ds(NT * q, NT)].astype(F32).reshape(192, 128) for q in range(NX)
@@ -278,6 +274,9 @@
     proj_in[kv] = proj_out[kv]
     leaving.append((sq1.at[pl.ds(0, 7)], 4))
     leaving.append((proj_in.at[pl.ds(0, 31)], 5))
+    for dy, dc in ALONG_Y:
+        copy_to(w_out.at[t], w_out.at[t], 3, kv, ts[dy][dc]).start()
+    leaving.append((w_out.at[pl.ds(0, 7)], 3))
     for dp, dx in PAIR:
         cols = units_of(xs[dx], pair_odd[dp])
         copy_to(wup_v.at[:, cols], w_up.at[y, in_pair], 6, pair_kvs[dp][dx], t).start()

time: 54.8 us -> 54.8 us (level)
  no operation moved by 1% of the time
where the time goes in v9:
time: 54.8 us; the launch traced here: 54.6 us
  Pallas kernels  54 us (99%)
  between operations  0.64 us (1%)
    pallas_call x1, Pallas kernels, body(): pl.pallas_call(kernel, out_shape=(jax.ShapeDtypeStruct(tokens.shape, toke...  52.8 us
    pallas_call x1, Pallas kernels, body(): pl.pallas_call(place, out_shape=(jax.ShapeDtypeStruct(out.shape, out.dtyp...  1.2 us

profile of v9, /device:TPU:1, one launch (start us, length us, event | category | flops | bytes accessed | tf_op | source)
XLA Modules:
  0.0 54.6 jit_solution(2548086170727121273)
XLA Ops:
  0.6 52.8 %decode_layer.1 = (bf16[48,64]{1,0:T(8,128)(2,1)S(1)}, f32[12,2,128,128]{3,2,1,0:T(8,128)S(1)}) custom-call(bf16[48,64]{1,0:T(8,128)(2,1)} %tokens_hbm.1, f32[1,64]{1,0:T(1,128)} %bitcast.8, f32[1,64]{1,0:T(1,128)} %bitcast.9, bf16[64,256]{1,0:T(8,128)(2,1)} %wq_hbm.1, bf16[64,256]{1,0:T(8,128)(2,1)} %wf_hbm.1, bf16[64,256]{1,0:T(8,128)(2,1)} %wi_hbm.1, ...), custom_call_target="tpu_custom_call" | custom-call | tf_op jit(solution)/shard_map/decode_layer/pallas_call | solution.py:480
  53.4 1.2 %place_outputs.1 = (bf16[48,64]{1,0:T(8,128)(2,1)}, f32[12,2,128,128]{3,2,1,0:T(8,128)}) custom-call(bf16[48,64]{1,0:T(8,128)(2,1)S(1)} %get-tuple-element.4.out_v, f32[12,2,128,128]{3,2,1,0:T(8,128)S(1)} %get-tuple-element.5.next_v), custom_call_target="tpu_custom_call" | custom-call | tf_op jit(solution)/shard_map/place_outputs/pallas_call | solution.py:540
